TPU v7x, 256 devices: a whole 4x4x8 slice. The times are simulated.
256 devices in a mesh: gr: 2 (over z_hi), fs: 16 (over z_lo, y), tp: 8 (over x, core).
Axes of the slice: x: 4, y: 4, z: 8 (z_hi: 2, z_lo: 4; z = z_hi * 4 + z_lo), core: 2. Of those that a mesh axis runs over, the one named last changes fastest.
Arguments:
- tokens: bfloat16 [8192, 2048], P(('gr', 'tp'), 'fs'), may hold values from -6 to 6
- routes: int32 [8192, 2], P(('gr', 'tp')), may hold values from 0 to 7, all different within a row; in each aligned block of 512 rows (0 to 511, 512 to 1023, ...) at most 192 rows name the same one
- route_weight: float32 [8192, 2], P(('gr', 'tp')), may hold values from 0.25 to 1
- norm_gain: float32 [2048], P(('gr', 'fs')), may hold values from 0.1 to 1.9
- gate_master: float32 [8, 2048, 2816], P(None, ('gr', 'fs'), 'tp'), may hold values from -0.125 to 0.125
- up_master: float32 [8, 2048, 2816], P(None, ('gr', 'fs'), 'tp'), may hold values from -0.125 to 0.125
- down_master: float32 [8, 2048, 2816], P(None, ('gr', 'fs'), 'tp'), may hold values from -0.109375 to 0.109375
Outputs:
- mixed_output: bfloat16 [8192, 2048], P(('gr', 'tp'), 'fs')
- gate_serving: bfloat16 [8, 2048, 2816], P('tp', None, 'fs')
- up_serving: bfloat16 [8, 2048, 2816], P('tp', None, 'fs')
- down_serving: bfloat16 [8, 2048, 2816], P('tp', None, 'fs')
Inputs may be any that keep to these rules, and one draw needn't show every extreme that they name: `routes`: each row names two different experts. Within the rows of one block of 512 tokens (one index of gr+tp) no expert is named by more than 192 rows, and in some blocks one expert is named by exactly 192.
All inputs are finite; a program needn't handle non-finite values.
Results may differ from a plain program's by a relative error of at most 0.0082.
Values may be sent and summed in bfloat16 or wider, within the bound.
A program may use at most 128 MiB of HBM per device.

v0:
```python
import jax
import jax.numpy as jnp
from jax import lax
from jax.sharding import PartitionSpec as P

norm_eps = 1e-06


def sent_together(arrays, axis, split_dim, concat_dim, along):
    ends, at = ([], 0)
    for a in arrays[:-1]:
        at += a.shape[along]
        ends.append(at)
    both = jnp.concatenate(arrays, axis=along)
    return tuple(
        jnp.split(
            lax.all_to_all(both, axis, split_axis=split_dim, concat_axis=concat_dim, tiled=True),
            ends,
            axis=along,
        )
    )


def copy_for_each(shard, axis):
    devices = lax.axis_size(axis)
    return lax.all_to_all(
        jnp.broadcast_to(shard[None], (devices, *shard.shape)), axis, 0, 0, tiled=True
    )


def in_order(parts, dim):
    parts = jnp.moveaxis(parts, 0, dim)
    dims = parts.shape
    return parts.reshape(*dims[:dim], dims[dim] * dims[dim + 1], *dims[dim + 2 :])


def gathered_copies(shard, axis, dim):
    parts = copy_for_each(shard, axis)
    return in_order(parts, dim)


def sent_together_2(arrays, axis, dim, along):
    widths = [a.shape[along] for a in arrays]
    both = jnp.concatenate(arrays, axis=along)
    out = gathered_copies(both, axis, dim)
    return tuple(jnp.split(out, [sum(widths[:k]) for k in range(1, len(widths))], axis=along))


def of_everyone(shard, axis):
    return copy_for_each(shard, axis).sum(axis=0)


def slot_table(routes, experts, capacity):
    flat_routes = routes.reshape(-1)
    onehot = (flat_routes[:, None] == jnp.arange(experts, dtype=jnp.int32)[None, :]).astype(
        jnp.int32
    )
    running = jnp.cumsum(onehot, axis=0)
    slot_index = jnp.sum(onehot * (running - 1), axis=1)
    return flat_routes * capacity + slot_index


def spread(gate_w, up_w, down_w):
    gate_e, up_e, down_e = sent_together((gate_w, up_w, down_w), "tp", 0, 2, 1)
    return sent_together((gate_e, up_e, down_e), "fs", 2, 1, 0)


def local(tokens, routes, route_weight, norm_gain, gate_master, up_master, down_master):
    experts = gate_master.shape[0]
    tp_count = lax.axis_size("tp")
    fs_count = lax.axis_size("fs")
    local_experts = experts // tp_count
    token_rows = tokens.shape[0]
    model_width = tokens.shape[1] * fs_count
    capacity = 3 * token_rows // experts
    scaled_gain = norm_gain[None, :, None]
    gate_w = (gate_master * scaled_gain).astype(jnp.bfloat16)
    up_w = (up_master * scaled_gain).astype(jnp.bfloat16)
    down_w = down_master.astype(jnp.bfloat16)
    gate_w, up_w, down_w = spread(gate_w, up_w, down_w)
    gate_w, up_w, down_w = sent_together_2((gate_w, up_w, down_w), "gr", 1, 0)
    as_float = tokens.astype(jnp.float32)
    square_total = of_everyone(jnp.sum(as_float * as_float, axis=1), "fs")
    normed = (as_float * lax.rsqrt(square_total / model_width + norm_eps)[:, None]).astype(
        jnp.bfloat16
    )
    placing = slot_table(routes, experts, capacity)
    slot_rows = jnp.arange(experts * capacity, dtype=jnp.int32)
    picked = (slot_rows[:, None] == placing[None, :]).reshape(experts * capacity, token_rows, 2)
    route_table = jnp.sum(picked.astype(jnp.float32), axis=2).astype(jnp.bfloat16)
    outgoing = jnp.dot(route_table, normed, preferred_element_type=jnp.float32).astype(jnp.bfloat16)
    outgoing = outgoing.reshape(tp_count, local_experts, capacity, tokens.shape[1])
    shard_piece = lax.all_gather(
        lax.all_to_all(outgoing, "tp", split_axis=0, concat_axis=0, tiled=True),
        "fs",
        axis=3,
        tiled=True,
    )
    gate_acc = jnp.einsum("sjcd,jdf->sjcf", shard_piece, gate_w, preferred_element_type=jnp.float32)
    up_acc = jnp.einsum("sjcd,jdf->sjcf", shard_piece, up_w, preferred_element_type=jnp.float32)
    gate_acc, up_acc = (gate_acc, up_acc)
    hidden = (jax.nn.silu(gate_acc) * up_acc).astype(jnp.bfloat16)
    partial_value = jnp.einsum("sjcf,jdf->sjcd", hidden, down_w, preferred_element_type=jnp.float32)
    summed = lax.psum_scatter(partial_value, "fs", scatter_dimension=3, tiled=True)
    produced = lax.all_to_all(summed, "tp", split_axis=0, concat_axis=0, tiled=True)
    produced = produced.reshape(experts * capacity, produced.shape[3])
    pair_slots = placing.reshape(token_rows, 2)
    first_rows = jnp.take(produced, pair_slots[:, 0], axis=0)
    second_rows = jnp.take(produced, pair_slots[:, 1], axis=0)
    mixed_out = first_rows * route_weight[:, 0:1] + second_rows * route_weight[:, 1:2]
    return (mixed_out.astype(jnp.bfloat16), gate_w, up_w, down_w)


def solution(mesh):
    placed = (
        P(("gr", "tp"), "fs"),
        P(("gr", "tp"), None),
        P(("gr", "tp"), None),
        P(("gr", "fs")),
        P(None, ("gr", "fs"), "tp"),
        P(None, ("gr", "fs"), "tp"),
        P(None, ("gr", "fs"), "tp"),
    )
    return jax.shard_map(
        local,
        mesh=mesh,
        in_specs=placed,
        out_specs=(
            P(("gr", "tp"), "fs"),
            P("tp", None, "fs"),
            P("tp", None, "fs"),
            P("tp", None, "fs"),
        ),
        check_vma=False,
    )
```

profile of v0, /device:TPU:64, one launch (start us, length us, event | category | flops | bytes accessed | tf_op | source)
XLA Modules:
  0.0 401.7 jit_solution(3067167331922924590)
XLA Ops:
  8.9 8.2 %all-to-all-start.3 = ((f32[16,1,512]{2,1,0:T(1,128)}), f32[16,1,512]{2,1,0:T(1,128)S(1)}, u32[]{:S(2)}, u32[]{:S(2)}) async-start(f32[16,1,512]{2,1,0:T(1,128)} %broadcast_in_dim.11), calls=%async_computation.3 | async-start | bytes 65536 | tf_op jit(solution)/shard_map/all_to_all | solution.py:26
  18.3 2.3 reduce-window.6
  21.5 1.5 convert_reduce_fusion
  23.8 13.2 %all_to_all.54 = bf16[8,1,192,128]{3,2,1,0:T(8,128)(2,1)} all-to-all(bf16[8,1,192,128]{3,2,1,0:T(8,128)(2,1)S(1)} %bitcast.109), channel_id=1, replica_groups=mesh['gr'=2,'fs'=16,'tp'=8] {'tp'}, dimensions={0} | all-to-all | bytes 786432 | tf_op jit(solution)/shard_map/all_to_all | solution.py:94
  37.6 19.8 %all_to_all.55 = bf16[8,192,352]{2,1,0:T(8,128)(2,1)S(1)} all-to-all(bf16[8,192,352]{2,1,0:T(8,128)(2,1)S(1)} %pad_maximum_fusion.1), channel_id=1, replica_groups=mesh['gr'=2,'fs'=16,'tp'=8] {'tp'}, dimensions={0} | all-to-all | bytes 2162688 | tf_op jit(solution)/shard_map/all_to_all | solution.py:17
  60.3 4.4 %copy.114 = bf16[3,64,2816]{1,0,2:T(4,128)(2,1)S(1)} copy(bf16[3,64,2816]{2,1,0:T(8,128)(2,1)} %pad_maximum_fusion.2) | data formatting | bytes 2162688 | tf_op jit(solution)/shard_map/concatenate | solution.py:14
  64.7 2.9 reshape.137
  67.6 52.4 %all_to_all.56 = bf16[16,2,16896]{2,1,0:T(2,128)(2,1)} all-to-all(bf16[16,2,16896]{2,1,0:T(2,128)(2,1)} %reshape.137), channel_id=1, replica_groups=mesh['gr'=2,'fs'=16,'tp'=8] {'fs'}, dimensions={0} | all-to-all | bytes 2162688 | tf_op jit(solution)/shard_map/all_to_all | solution.py:17
  120.0 5.3 %reshape.138 = bf16[2816,3,64]{2,1,0:T(4,128)(2,1)S(1)} reshape(bf16[16,2,16896]{2,1,0:T(2,128)(2,1)} %all_to_all.56) | data formatting | bytes 2162688
  125.3 4.0 %copy.130 = bf16[3,64,16,176]{3,2,1,0:T(8,128)(2,1)} copy(bf16[3,64,16,176]{1,0,3,2:T(4,128)(2,1)S(1)} %bitcast.100) | data formatting | bytes 2162688 | tf_op jit(solution)/shard_map/all_to_all | solution.py:17
  129.3 1.5 fusion.33
  132.7 56.5 %all_to_all.57 = bf16[2,3,1024,176]{2,3,1,0:T(8,128)(2,1)S(1)} all-to-all(bf16[2,3,1024,176]{2,3,1,0:T(8,128)(2,1)S(1)} %broadcast_in_dim.10), channel_id=1, replica_groups=mesh['gr'=2,'fs'=16,'tp'=8] {'gr'}, dimensions={0} | all-to-all | bytes 4325376 | tf_op jit(solution)/shard_map/all_to_all | solution.py:26
  189.2 1.4 slice_bitcast_fusion.2
  190.5 1.6 copy.121
  192.1 3.1 reshape.130
  195.2 2.7 copy.125
  197.9 3.1 reshape.131
  201.0 1.6 copy.120
  202.6 3.1 reshape.132
  205.7 6.0 %fusion.5 = f32[8,1,192,176]{2,3,0,1:T(8,128)} fusion(bf16[2048,176,1]{0,1,2:T(8,128)(2,1)} %reshape.130, bf16[8,1,192,2048]{3,2,0,1:T(8,128)(2,1)} %all-gather.2.cloned.1.call-done), kind=kOutput, calls=%fused_computation.12 | convolution fusion | flops 1107296256 | bytes 8093696 | tf_op jit(solution)/shard_map/sjcd,jdf->sjcf/dot_general | solution.py:99
  211.7 11.5 %convolution_bitcast_fusion = f32[8,1,192,2048]{3,2,0,1:T(8,128)} fusion(bf16[2048,176,1]{0,1,2:T(8,128)(2,1)} %reshape.132, bf16[2048,176,1]{0,1,2:T(8,128)(2,1)S(1)} %copy-done, bf16[8,1,192,2048]{3,2,0,1:T(8,128)(2,1)} %all-gather.2.cloned.1.call-done, f32[8,1,192,176]{2,3,0,1:T(8,128)} %fusion.5), kind=kOutput, calls=%fused_computation.8 | convolution fusion | flops 2216214528 | bytes 21397504 | tf_op jit(solution)/shard_map/sjcf,jdf->sjcd/dot_general | solution.py:103
  223.2 151.2 %reduce-scatter.2.cloned.1.call-done = f32[8,1,192,128]{3,2,0,1:T(8,128)} async-done(((f32[8,1,192,2048]{3,2,0,1:T(8,128)}), f32[8,1,192,128]{3,2,0,1:T(8,128)}) %reduce-scatter.2.cloned.1.call-update) | async-done | bytes 786448 | tf_op jit(solution)/shard_map/reduce_scatter | solution.py:104
  374.4 4.3 %all-to-all-start.5 = ((f32[8,1,192,128]{3,2,1,0:T(8,128)}), f32[8,1,192,128]{3,2,1,0:T(8,128)S(1)}, u32[]{:S(2)}, u32[]{:S(2)}) async-start(f32[8,1,192,128]{3,2,1,0:T(8,128)} %bitcast.110), calls=%async_computation.6 | async-start | bytes 1572864 | tf_op jit(solution)/shard_map/all_to_all | solution.py:105
  381.5 10.3 %all-to-all-done.5 = f32[8,1,192,128]{3,2,1,0:T(8,128)S(1)} async-done(((f32[8,1,192,128]{3,2,1,0:T(8,128)}), f32[8,1,192,128]{3,2,1,0:T(8,128)S(1)}, u32[]{:S(2)}, u32[]{:S(2)}) %all-to-all-start.5) | async-done | bytes 786464 | tf_op jit(solution)/shard_map/all_to_all | solution.py:105
  (64 shorter events, 15.6 us)
Async XLA Ops:
  7.2 14.3 %copy-start.5 = (s32[512,2]{0,1:T(2,128)S(1)}, s32[512,2]{0,1:T(2,128)}, u32[]{:S(2)}) copy-start(s32[512,2]{0,1:T(2,128)} %param.10) | copy-start | bytes 12292
  8.9 14.2 %all-to-all-start.3 = ((f32[16,1,512]{2,1,0:T(1,128)}), f32[16,1,512]{2,1,0:T(1,128)S(1)}, u32[]{:S(2)}, u32[]{:S(2)}) async-start(f32[16,1,512]{2,1,0:T(1,128)} %broadcast_in_dim.11), calls=%async_computation.3 | async-start | bytes 65536 | tf_op jit(solution)/shard_map/all_to_all | solution.py:26
  17.1 6.0 %copy-start.4 = (bf16[512,128]{1,0:T(8,128)(2,1)S(1)}, bf16[512,128]{1,0:T(8,128)(2,1)}, u32[]{:S(2)}) copy-start(bf16[512,128]{1,0:T(8,128)(2,1)} %param.9) | copy-start | bytes 393220
  17.1 188.6 %all-gather.2.cloned.1.call-start = ((), (), s32[]{:S(2)}) async-start(), calls=%async_computation.7 | async-start | bytes 6684672 | tf_op jit(solution)/shard_map/all_gather | solution.py:93
  23.1 14.0 %copy-start.3 = (f32[8,64,352]{2,1,0:T(8,128)S(1)}, f32[8,64,352]{2,1,0:T(8,128)}, u32[]{:S(2)}) copy-start(f32[8,64,352]{2,1,0:T(8,128)} %param.15) | copy-start | bytes 2162692
  23.8 13.4 %copy-start.1 = (f32[8,64,352]{2,1,0:T(8,128)S(1)}, f32[8,64,352]{2,1,0:T(8,128)}, u32[]{:S(2)}) copy-start(f32[8,64,352]{2,1,0:T(8,128)} %param.13) | copy-start | bytes 2162692
  23.8 13.4 %copy-start.2 = (f32[8,64,352]{2,1,0:T(8,128)S(1)}, f32[8,64,352]{2,1,0:T(8,128)}, u32[]{:S(2)}) copy-start(f32[8,64,352]{2,1,0:T(8,128)} %param.14) | copy-start | bytes 2162692
  23.8 13.4 %copy-start.7 = (f32[64]{0:T(128)S(1)}, f32[64]{0:T(128)}, u32[]{:S(2)}) copy-start(f32[64]{0:T(128)} %param.12) | copy-start | bytes 772
  37.1 337.3 %reduce-scatter.2.cloned.1.call-start = ((), (), s32[]{:S(2)}) async-start(), calls=%async_computation.8 | async-start | bytes 13369344 | tf_op jit(solution)/shard_map/reduce_scatter | solution.py:104
  205.7 6.0 %copy-start = (bf16[2048,176,1]{0,1,2:T(8,128)(2,1)S(1)}, bf16[2048,176,1]{0,1,2:T(8,128)(2,1)}, u32[]{:S(2)}) copy-start(bf16[2048,176,1]{0,1,2:T(8,128)(2,1)} %reshape.131) | copy-start | bytes 2162692
  223.2 155.5 %copy-start.6 = (f32[512,2]{0,1:T(2,128)S(1)}, f32[512,2]{0,1:T(2,128)}, u32[]{:S(2)}) copy-start(f32[512,2]{0,1:T(2,128)} %param.11) | copy-start | bytes 12292
  374.4 17.4 %all-to-all-start.5 = ((f32[8,1,192,128]{3,2,1,0:T(8,128)}), f32[8,1,192,128]{3,2,1,0:T(8,128)S(1)}, u32[]{:S(2)}, u32[]{:S(2)}) async-start(f32[8,1,192,128]{3,2,1,0:T(8,128)} %bitcast.110), calls=%async_computation.6 | async-start | bytes 1572864 | tf_op jit(solution)/shard_map/all_to_all | solution.py:105
Sparse Core Ops, SparseCore 0:
  37.2 146.7 all-gather.1
  223.3 151.0 reduce-scatter.1
where the time goes:
time: 407 us; the launch traced here: 402 us
  waiting for transfers between devices  161 us (40%)
  blocking collectives  142 us (35%)
  local copies, waits for them, and re-layouts  45.2 us (11%)
  matrix products  18.1 us (4%)
  between operations  14.4 us (4%)
  starting transfers between devices  12.5 us (3%)
  other arithmetic  8.05 us (2%)
    reduce_scatter x1, waiting for transfers between devices, local(): lax.psum_scatter(partial_value, 'fs', scatter_dimension=3, tiled=True)  151 us
    all_to_all x2, blocking collectives, sent_together(): lax.all_to_all(both, axis, split_axis=split_dim, concat_axis=concat_dim,...  72.2 us
    all_to_all x1, blocking collectives, copy_for_each(): lax.all_to_all(jnp.broadcast_to(shard[None], (devices, *shard.shape)), ax...  56.5 us
    all_to_all x1, blocking collectives, local(): lax.all_to_all(outgoing, 'tp', split_axis=0, concat_axis=0, tiled=True)  13.2 us
    dot_general x1, matrix products, local(): jnp.einsum('sjcf,jdf->sjcd', hidden, down_w, preferred_element_type=jnp.f...  11.5 us
    unnamed x20, local copies, waits for them, and re-layouts  10.4 us
    all_to_all x1, waiting for transfers between devices, local(): lax.all_to_all(summed, 'tp', split_axis=0, concat_axis=0, tiled=True)  10.3 us
    another operation x3, local copies, waits for them, and re-layouts  9.23 us
  transfers between devices with their start and end apart: 4, of which 2 were waited for; matrix products, arithmetic and copies ran while one was open for 12% of the time, Pallas kernels for 0%

commit v1 on v0

v1 whole, which is shorter than its diff:
```python
import jax
import jax.numpy as jnp
from jax import lax
from jax.experimental import pallas as pl
from jax.experimental.pallas import tpu as pltpu
from jax.sharding import PartitionSpec as P

norm_eps = 1e-06
BF = jnp.bfloat16
F32 = jnp.float32
I32 = jnp.int32
MESH = pl.DeviceIdType.MESH
VMEM_LIMIT = 60 * 1024 * 1024

NY, NZ, NX, NC = 4, 4, 4, 2
NT = NX * NC
EXPERTS = 8
CAP = 192
ROWS = 64
COLS = 176
LANES = 128
TAIL = COLS - LANES
PACK = 3 * ROWS + ROWS + 16
TOK = 512
FEAT = 128
ZF = NZ * FEAT
KS = (4, 3, 5, 2, 6, 1, 7, 0)


def coords():
    g, f, t = lax.axis_index("gr"), lax.axis_index("fs"), lax.axis_index("tp")
    return g, lax.div(f, NY), lax.rem(f, NY), t


def at(g, z, y, t):
    return (g, z * NY + y, t)


def rem(a, n):
    return lax.rem(a, n)


def send(src, dst, ss, rs, to):
    return pltpu.make_async_remote_copy(
        src_ref=src, dst_ref=dst, send_sem=ss, recv_sem=rs, device_id=to, device_id_type=MESH
    )


def slot_keys(routes_ref):
    ex = lax.broadcasted_iota(I32, (16, TOK), 0)
    named = (routes_ref[0:1, :] == ex) | (routes_ref[1:2, :] == ex)
    ones = jnp.where(named, 1.0, 0.0).astype(BF)
    before = lax.broadcasted_iota(I32, (TOK, TOK), 0) < lax.broadcasted_iota(I32, (TOK, TOK), 1)
    rank = jnp.dot(ones, jnp.where(before, 1.0, 0.0).astype(BF), preferred_element_type=F32)
    return jnp.where(named, rank, -1.0)


def gather_kernel(
    tok_ref, routes_ref, gain_ref, gm_ref, um_ref, dm_ref,
    v_ref, x_ref,
    key_ref, wp_ref, q_ref, t_ref, s_ref,
    zs, zr, qs, qr, vs, vr, xs, xr, ys, yr,
):
    g, z, y, t = coords()
    x, c = lax.div(t, NC), lax.rem(t, NC)
    up_y, dn_y = rem(y + 1, NY), rem(y + NY - 1, NY)

    barrier = pltpu.get_barrier_semaphore()
    count = 0
    for dy in range(NY):
        for dt in range(NT):
            if dy or dt:
                pl.semaphore_signal(barrier, inc=1, device_id=at(g, z, rem(y + dy, NY), rem(t + dt, NT)), device_id_type=MESH)
                count += 1
    for dg in range(2):
        for dz in range(NZ):
            if dg or dz:
                pl.semaphore_signal(barrier, inc=1, device_id=at(rem(g + dg, 2), rem(z + dz, NZ), y, t), device_id_type=MESH)
                count += 1

    gain = gain_ref[...]
    for k in KS:
        e = rem(t + k, NT)
        gw, uw, dw = gm_ref[e] * gain, um_ref[e] * gain, dm_ref[e]
        for h in range(2):
            lo = h * COLS
            for j, w in enumerate((gw, uw, dw)):
                wp_ref[k, h, j * ROWS:(j + 1) * ROWS, :] = w[:, lo:lo + LANES].astype(BF)
            gt, ut, dt_ = (w[:, lo + LANES:lo + COLS] for w in (gw, uw, dw))
            wp_ref[k, h, 3 * ROWS:4 * ROWS, :] = jnp.concatenate([gt, ut, dt_[:, :32]], axis=1).astype(BF)
            rest = dt_[:, 32:48]
            extra = jnp.concatenate([rest[8 * i:8 * i + 8] for i in range(8)], axis=1)
            wp_ref[k, h, 4 * ROWS:4 * ROWS + 16, :] = jnp.concatenate([extra, jnp.zeros_like(extra)], axis=0).astype(BF)
    key_ref[...] = slot_keys(routes_ref)

    pl.semaphore_wait(barrier, count)

    tok_sends = []
    for j in (3, 2, 1):
        d = send(tok_ref, t_ref.at[z], zs.at[j], zr.at[j], at(g, rem(z + j, NZ), y, t))
        d.start()
        tok_sends.append(d)
    own_tok = pltpu.make_async_copy(tok_ref, t_ref.at[z], zr.at[0])
    own_tok.start()

    def first(k, h):
        return send(
            wp_ref.at[k, h], q_ref.at[x, y], qs.at[k, h], qr.at[x * NY + y],
            at(g, z, NC * c + h, rem(t + k, NT)),
        )

    def first_own(h):
        return pltpu.make_async_copy(wp_ref.at[0, h], q_ref.at[x, y], qr.at[x * NY + y])

    for k in KS:
        for h in range(2):
            if k:
                first(k, h).start()
            else:
                mine = NC * c + h == y

                @pl.when(mine)
                def _():
                    first_own(h).start()

                @pl.when(jnp.logical_not(mine))
                def _():
                    first(k, h).start()

    own_tok.wait()
    for j in (1, 2, 3):
        tok_sends[3 - j].wait_recv()
    rows_in = jnp.concatenate([t_ref[i] for i in range(NZ)], axis=1)
    slot = lax.broadcasted_iota(I32, (CAP, TOK), 0).astype(F32)
    for k in KS:
        key = key_ref[pl.ds(rem(t + k, NT), 1), :]
        table = jnp.where(slot == key, 1.0, 0.0).astype(BF)
        s_ref[k] = jnp.dot(table, rows_in, preferred_element_type=F32).astype(BF)

    def across(k):
        return send(s_ref.at[k], x_ref.at[t, y], xs.at[k], xr.at[k], at(g, z, y, rem(t + k, NT)))

    own_rows = pltpu.make_async_copy(s_ref.at[0], x_ref.at[t, y], xr.at[0])
    own_rows.start()
    for k in KS[:-1]:
        across(k).start()

    zz = g * NZ + z

    def second(j, q):
        zd = rem(z + j, NZ)
        return send(q_ref.at[zd], v_ref.at[zz], vs.at[j, q], vr.at[j, q], at(rem(g + q, 2), zd, y, t))

    own_v = pltpu.make_async_copy(q_ref.at[z], v_ref.at[zz], vr.at[0, 0])
    for j in (2, 1, 3, 0):
        zd = rem(z + j, NZ)
        for i in range(NY):
            send(wp_ref.at[0, 0], q_ref.at[zd, i], qs.at[0, 0], qr.at[zd * NY + i], at(g, z, up_y, t)).wait_recv()
        for q in (1, 0):
            if j or q:
                second(j, q).start()
            else:
                own_v.start()

    def block(k):
        return rem(t + NT - k, NT)

    def along(k, way):
        b = block(k)
        if way == 0:
            return send(x_ref.at[b, y], x_ref.at[b, y], ys.at[k, 0], yr.at[k, 0], at(g, z, up_y, t))
        if way == 1:
            return send(x_ref.at[b, y], x_ref.at[b, y], ys.at[k, 1], yr.at[k, 1], at(g, z, dn_y, t))
        if k % 2 == 0:
            return send(x_ref.at[b, dn_y], x_ref.at[b, dn_y], ys.at[k, 2], yr.at[k, 2], at(g, z, up_y, t))
        return send(x_ref.at[b, up_y], x_ref.at[b, up_y], ys.at[k, 2], yr.at[k, 2], at(g, z, dn_y, t))

    order = (0, 1, 7, 2, 6, 3, 5, 4)
    for i, k in enumerate(order):
        if k:
            across(k).wait_recv()
        else:
            own_rows.wait()
        along(k, 0).start()
        along(k, 1).start()
        if i >= 2:
            p = order[i - 2]
            along(p, p % 2).wait_recv()
            along(p, 2).start()
    for p in order[-2:]:
        along(p, p % 2).wait_recv()
        along(p, 2).start()

    for k in order:
        along(k, 1 - k % 2).wait_recv()
        along(k, 2).wait_recv()
        for way in range(3):
            along(k, way).wait_send()
        if k:
            across(k).wait_send()
    own_v.wait()
    for j in range(NZ):
        for q in range(2):
            if j or q:
                second(j, q).wait()
    for d in tok_sends:
        d.wait_send()
    for k in KS:
        for h in range(2):
            if k:
                first(k, h).wait_send()
            else:
                @pl.when(NC * c + h != y)
                def _():
                    first(k, h).wait_send()


def expert_kernel(v_ref, x_ref, gate_ref, up_ref, down_ref, p_ref):
    @pl.when(pl.program_id(0) == 0)
    def _():
        lane = lax.broadcasted_iota(I32, (ROWS, LANES), 1)

        def piece(i, _):
            zi, yi = lax.div(i, NY), lax.rem(i, NY)
            rows = pl.ds(pl.multiple_of(i * ROWS, ROWS), ROWS)
            for j, w in enumerate((gate_ref, up_ref, down_ref)):
                w[0, rows, 0:LANES] = v_ref[zi, yi, j * ROWS:(j + 1) * ROWS, :]
            tails = v_ref[zi, yi, 3 * ROWS:4 * ROWS, :].astype(F32)
            extra = v_ref[zi, yi, 4 * ROWS:4 * ROWS + 16, :].astype(F32)[0:8]
            rest = jnp.concatenate([pltpu.roll(extra, (32 + LANES - 16 * n) % LANES, 1) for n in range(8)], axis=0)
            gate_ref[0, rows, LANES:COLS] = tails[:, 0:TAIL].astype(BF)
            up_ref[0, rows, LANES:COLS] = pltpu.roll(tails, LANES - TAIL, 1)[:, 0:TAIL].astype(BF)
            down_tail = jnp.where(lane < 32, pltpu.roll(tails, LANES - 2 * TAIL, 1), rest)
            down_ref[0, rows, LANES:COLS] = down_tail[:, 0:TAIL].astype(BF)
            return 0

        lax.fori_loop(0, 2 * NZ * NY, piece, 0)

    rows = jnp.concatenate(
        [x_ref[0, yi, :, zi * FEAT:(zi + 1) * FEAT] for zi in range(NZ) for yi in range(NY)], axis=1
    )
    wide = rows.astype(F32)
    scale = lax.rsqrt(jnp.sum(wide * wide, axis=1, keepdims=True) / (NZ * NY * FEAT) + norm_eps)
    gate = jnp.dot(rows, gate_ref[0], preferred_element_type=F32) * scale
    up = jnp.dot(rows, up_ref[0], preferred_element_type=F32) * scale
    hidden = (gate / (1.0 + jnp.exp(-gate)) * up).astype(BF)
    out = lax.dot_general(hidden, down_ref[0], (((1,), (1,)), ((), ())), preferred_element_type=F32).astype(BF)
    for zi in range(NZ):
        for yi in range(NY):
            f = zi * NY + yi
            p_ref[0, yi, :, zi * FEAT:(zi + 1) * FEAT] = out[:, f * FEAT:(f + 1) * FEAT]


def reduce_kernel(
    p_ref, routes_ref, weight_ref,
    out_ref,
    key_ref, mix_ref, r_ref, a_ref, u_ref, w_ref, o_ref, e_ref, m_ref, l_ref,
    rs, rr, us, ur, ws, wr, os, orr, zs, zr,
):
    g, z, y, t = coords()
    up_y, dn_y, far_y = rem(y + 1, NY), rem(y + NY - 1, NY), rem(y + 2, NY)

    barrier = pltpu.get_barrier_semaphore()
    count = 0
    for to in (
        [at(g, z, up_y, t), at(g, z, dn_y, t)]
        + [at(g, z, y, rem(t + k, NT)) for k in range(1, NT)]
        + [at(g, rem(z + j, NZ), y, t) for j in range(1, NZ)]
    ):
        pl.semaphore_signal(barrier, inc=1, device_id=to, device_id_type=MESH)
        count += 1

    keys = slot_keys(routes_ref)
    key_ref[...] = keys
    ex = lax.broadcasted_iota(I32, (16, TOK), 0)
    mix_ref[...] = jnp.where(routes_ref[0:1, :] == ex, weight_ref[0:1, :], 0.0) + jnp.where(
        routes_ref[1:2, :] == ex, weight_ref[1:2, :], 0.0
    )
    pl.semaphore_wait(barrier, count)

    def block(k):
        return rem(t + k, NT)

    def near(k):
        return up_y if k % 2 == 0 else dn_y

    def other(k):
        return dn_y if k % 2 == 0 else up_y

    def far(k):
        return send(p_ref.at[block(k), far_y], r_ref.at[k], rs.at[k], rr.at[k], at(g, z, near(k), t))

    def plain(k):
        return send(p_ref.at[block(k), other(k)], u_ref.at[k], us.at[k], ur.at[k], at(g, z, other(k), t))

    def summed(k):
        return send(a_ref.at[k], w_ref.at[k], ws.at[k], wr.at[k], at(g, z, near(k), t))

    def back(k):
        return send(o_ref.at[k], e_ref.at[t], os.at[k], orr.at[k], at(g, z, y, block(k)))

    for k in KS:
        far(k).start()
    for k in KS:
        plain(k).start()

    def finish(k):
        plain(k).wait_recv()
        summed(k).wait_recv()
        total = p_ref[block(k), y].astype(F32) + u_ref[k].astype(F32) + w_ref[k].astype(F32)
        if k:
            o_ref[k] = total.astype(BF)
            back(k).start()
        else:
            e_ref[t] = total.astype(BF)

    for i, k in enumerate(KS):
        far(k).wait_recv()
        a_ref[k] = (r_ref[k].astype(F32) + p_ref[block(k), near(k)].astype(F32)).astype(BF)
        summed(k).start()
        if i >= 2:
            finish(KS[i - 2])
    for k in KS[-2:]:
        finish(k)

    slot = lax.broadcasted_iota(I32, (CAP, TOK), 0).astype(F32)
    total = jnp.zeros((TOK, ZF), F32)
    for k in (0, 4, 5, 3, 6, 2, 7, 1):
        e = rem(t + NT - k, NT)
        if k:
            back(k).wait_recv()
        key, mix = key_ref[pl.ds(e, 1), :], mix_ref[pl.ds(e, 1), :]
        mix_hi = mix.astype(BF).astype(F32)
        here = slot == key
        produced = e_ref[e]
        for part in (mix_hi, mix - mix_hi):
            table = jnp.where(here, part, 0.0).astype(BF)
            total = total + lax.dot_general(table, produced, (((0,), (0,)), ((), ())), preferred_element_type=F32)
    for i in range(NZ):
        m_ref[i] = total[:, i * FEAT:(i + 1) * FEAT].astype(BF)

    def part(j):
        zd = rem(z + j, NZ)
        return send(m_ref.at[zd], l_ref.at[j], zs.at[j], zr.at[j], at(g, zd, y, t))

    for j in (3, 2, 1):
        part(j).start()
    own = m_ref[z].astype(F32)
    for j in (1, 2, 3):
        part(j).wait_recv()
        own = own + l_ref[j].astype(F32)
    out_ref[...] = own.astype(BF)

    for k in KS:
        far(k).wait_send()
        plain(k).wait_send()
        summed(k).wait_send()
        if k:
            back(k).wait_send()
    for j in (1, 2, 3):
        part(j).wait_send()


def local(tokens, routes, route_weight, norm_gain, gate_master, up_master, down_master):
    vm = pl.BlockSpec(memory_space=pltpu.VMEM)
    any_ = pl.BlockSpec(memory_space=pl.ANY)
    dma = pltpu.SemaphoreType.DMA
    routes_t = routes.T
    weight_t = route_weight.T
    v, rows = pl.pallas_call(
        gather_kernel,
        out_shape=(
            jax.ShapeDtypeStruct((2 * NZ, NY, PACK, LANES), BF),
            jax.ShapeDtypeStruct((NT, NY, CAP, ZF), BF),
        ),
        in_specs=[vm] * 6,
        out_specs=(any_, any_),
        scratch_shapes=[
            pltpu.VMEM((16, TOK), F32),
            pltpu.VMEM((NT, 2, PACK, LANES), BF),
            pltpu.VMEM((NX, NY, PACK, LANES), BF),
            pltpu.VMEM((NZ, TOK, FEAT), BF),
            pltpu.VMEM((NT, CAP, ZF), BF),
            dma((NZ,)), dma((NZ,)),
            dma((NT, 2)), dma((NX * NY,)),
            dma((NZ, 2)), dma((NZ, 2)),
            dma((NT,)), dma((NT,)),
            dma((NT, 3)), dma((NT, 3)),
        ],
        compiler_params=pltpu.CompilerParams(collective_id=0, has_side_effects=True, vmem_limit_bytes=VMEM_LIMIT),
        name="gather_kernel",
    )(tokens, routes_t, norm_gain[:, None], gate_master, up_master, down_master)

    serving = jax.ShapeDtypeStruct((1, 2048, COLS), BF)
    whole = pl.BlockSpec((1, 2048, COLS), lambda b: (0, 0, 0))
    per_block = pl.BlockSpec((1, NY, CAP, ZF), lambda b: (b, 0, 0, 0))
    gate_w, up_w, down_w, partial = pl.pallas_call(
        expert_kernel,
        grid=(NT,),
        out_shape=(serving, serving, serving, jax.ShapeDtypeStruct((NT, NY, CAP, ZF), BF)),
        in_specs=[pl.BlockSpec((2 * NZ, NY, PACK, LANES), lambda b: (0, 0, 0, 0)), per_block],
        out_specs=(whole, whole, whole, per_block),
        compiler_params=pltpu.CompilerParams(vmem_limit_bytes=VMEM_LIMIT),
        name="expert_kernel",
    )(v, rows)

    buf = pltpu.VMEM((NT, CAP, ZF), BF)
    mixed = pl.pallas_call(
        reduce_kernel,
        out_shape=jax.ShapeDtypeStruct((TOK, FEAT), BF),
        in_specs=[vm] * 3,
        out_specs=vm,
        scratch_shapes=[
            pltpu.VMEM((16, TOK), F32),
            pltpu.VMEM((16, TOK), F32),
            buf, buf, buf, buf, buf, buf,
            pltpu.VMEM((NZ, TOK, FEAT), BF),
            pltpu.VMEM((NZ, TOK, FEAT), BF),
            dma((NT,)), dma((NT,)), dma((NT,)), dma((NT,)), dma((NT,)), dma((NT,)), dma((NT,)), dma((NT,)),
            dma((NZ,)), dma((NZ,)),
        ],
        compiler_params=pltpu.CompilerParams(collective_id=1, has_side_effects=True, vmem_limit_bytes=VMEM_LIMIT),
        name="reduce_kernel",
    )(partial, routes_t, weight_t)
    return mixed, gate_w, up_w, down_w


def solution(mesh):
    placed = (
        P(("gr", "tp"), "fs"),
        P(("gr", "tp"), None),
        P(("gr", "tp"), None),
        P(("gr", "fs")),
        P(None, ("gr", "fs"), "tp"),
        P(None, ("gr", "fs"), "tp"),
        P(None, ("gr", "fs"), "tp"),
    )
    return jax.shard_map(
        local,
        mesh=mesh,
        in_specs=placed,
        out_specs=(
            P(("gr", "tp"), "fs"),
            P("tp", None, "fs"),
            P("tp", None, "fs"),
            P("tp", None, "fs"),
        ),
        check_vma=False,
    )
```

time: 407 us -> 195 us (0.48)
  the two profiles are of different devices: /device:TPU:64 before, /device:TPU:16 now
where the time goes in v1:
time: 195 us; the launch traced here: 194 us
  Pallas kernels  187 us (96%)
  local copies, waits for them, and re-layouts  6.57 us (3%)
    pallas_call x1, Pallas kernels, local(): pl.pallas_call(gather_kernel, out_shape=(jax.ShapeDtypeStruct((2 * NZ, NY...  89.6 us
    pallas_call x1, Pallas kernels, local(): pl.pallas_call(reduce_kernel, out_shape=jax.ShapeDtypeStruct((TOK, FEAT),...  82.1 us
    pallas_call x1, Pallas kernels, local(): pl.pallas_call(expert_kernel, grid=(NT,), out_shape=(serving, serving, se...  15.2 us
    unnamed x10, local copies, waits for them, and re-layouts  5.21 us

profile of v1, /device:TPU:16, one launch (start us, length us, event | category | flops | bytes accessed | tf_op | source)
XLA Modules:
  0.0 194.2 jit_solution(17236951925222142663)
XLA Ops:
  0.6 1.4 copy.11.gain_ref
  2.0 89.6 %gather_kernel.1 = (bf16[8,4,272,128]{3,2,1,0:T(8,128)(2,1)}, bf16[8,4,192,512]{3,2,1,0:T(8,128)(2,1)}) custom-call(bf16[512,128]{1,0:T(8,128)(2,1)} %tok_ref.1, s32[2,512]{1,0:T(2,128)} %bitcast.3, f32[64,1]{1,0:T(8,128)} %copy.11.gain_ref, f32[8,64,352]{2,1,0:T(8,128)} %gm_ref.1, f32[8,64,352]{2,1,0:T(8,128)} %um_ref.1, f32[8,64,352]{2,1,0:T(8,128)} %dm_ref.1), custom_call_target="tpu_custom_call" | custom-call | tf_op jit(solution)/shard_map/gather_kernel/pallas_call | solution.py:370
  91.6 15.2 %expert_kernel.1 = (bf16[1,2048,176]{2,1,0:T(8,128)(2,1)}, bf16[1,2048,176]{2,1,0:T(8,128)(2,1)}, bf16[1,2048,176]{2,1,0:T(8,128)(2,1)}, bf16[8,4,192,512]{3,2,1,0:T(8,128)(2,1)}) custom-call(bf16[8,4,272,128]{3,2,1,0:T(8,128)(2,1)} %get-tuple-element.10.v_ref, bf16[8,4,192,512]{3,2,1,0:T(8,128)(2,1)} %get-tuple-element.11.x_ref), custom_call_target="tpu_custom_call" | custom-call | tf_op jit(solution)/shard_map/expert_kernel/pallas_call | solution.py:397
  106.8 0.0 copy-start.2
  106.8 0.0 copy-start.1
  106.8 0.0 copy-start
  106.8 82.1 %reduce_kernel.1 = bf16[512,128]{1,0:T(8,128)(2,1)} custom-call(bf16[8,4,192,512]{3,2,1,0:T(8,128)(2,1)} %get-tuple-element.12.p_ref, s32[2,512]{1,0:T(2,128)} %bitcast.4, f32[2,512]{1,0:T(2,128)} %bitcast.5), custom_call_target="tpu_custom_call" | custom-call | tf_op jit(solution)/shard_map/reduce_kernel/pallas_call | solution.py:408
  188.9 0.0 copy-done.2
  189.0 1.2 copy.12
  190.2 0.0 copy-done.1
  190.2 1.2 copy.13
  191.4 0.0 copy-done
  191.4 1.2 copy.14
  192.6 1.6 copy.16
Async XLA Ops:
  106.8 82.1 %copy-start.2 = (bf16[1,2048,176]{2,1,0:T(8,128)(2,1)S(1)}, bf16[1,2048,176]{2,1,0:T(8,128)(2,1)}, u32[]{:S(2)}) copy-start(bf16[1,2048,176]{2,1,0:T(8,128)(2,1)} %get-tuple-element.17) | copy-start | bytes 2162692
  106.8 83.4 %copy-start.1 = (bf16[1,2048,176]{2,1,0:T(8,128)(2,1)S(1)}, bf16[1,2048,176]{2,1,0:T(8,128)(2,1)}, u32[]{:S(2)}) copy-start(bf16[1,2048,176]{2,1,0:T(8,128)(2,1)} %get-tuple-element.18) | copy-start | bytes 2162692
  106.8 84.6 %copy-start = (bf16[1,2048,176]{2,1,0:T(8,128)(2,1)S(1)}, bf16[1,2048,176]{2,1,0:T(8,128)(2,1)}, u32[]{:S(2)}) copy-start(bf16[1,2048,176]{2,1,0:T(8,128)(2,1)} %get-tuple-element.19) | copy-start | bytes 2162692

commit v2 on v0

v2 whole, which is shorter than its diff:
```python
import jax
import jax.numpy as jnp
from jax import lax
from jax.experimental import pallas as pl
from jax.experimental.pallas import tpu as pltpu
from jax.sharding import PartitionSpec as P

norm_eps = 1e-06
BF = jnp.bfloat16
F32 = jnp.float32
I32 = jnp.int32
MESH = pl.DeviceIdType.MESH
VMEM_LIMIT = 60 * 1024 * 1024

NY, NZ, NX, NC = 4, 4, 4, 2
NT = NX * NC
EXPERTS = 8
CAP = 192
ROWS = 64
WIDTH = 352
COLS = 176
LANES = 128
DLO, DHI = 96, 80
PACK = COLS + DLO
TOK = 512
FEAT = 128
MODEL = 2048
NEAR = (0, 1, 7, 2, 6, 3, 5, 4)
FARS = (4, 3, 5, 2, 6, 1, 7, 0)
HALVES = ((0, 3), (1, 2))


def rem(a, n):
    return lax.rem(a, n)


def at(g, z, y, t):
    return (g, z * NY + y, t)


def send(src, dst, ss, rs, to):
    return pltpu.make_async_remote_copy(
        src_ref=src, dst_ref=dst, send_sem=ss, recv_sem=rs, device_id=to, device_id_type=MESH
    )


def kernel(
    tok_ref, routes_ref, weight_ref, gain_ref, gm_hbm, um_hbm, dm_hbm,
    out_ref, gate_out, up_out, down_out,
    gm_ref, um_ref, dm_ref, key_ref, mix_ref, table_ref, comb_ref,
    wp_ref, q_ref, v_ref, t_ref, s_ref, x_ref, gate_ref, up_ref, down_ref, h_ref,
    p_ref, r_ref, a_ref, u_ref, w_ref, o_ref, e_ref, m_ref, l_ref,
    ms, zs, zr, qs, qr, vs, vr, xs, xr, ys, yr,
    fs, fr, us, ur, ws, wr, bs, br, cs, cr, outs,
):
    g, f, t = lax.axis_index("gr"), lax.axis_index("fs"), lax.axis_index("tp")
    z, y = lax.div(f, NY), rem(f, NY)
    x, c = lax.div(t, NC), rem(t, NC)
    up_y, dn_y, far_y = rem(y + 1, NY), rem(y + NY - 1, NY), rem(y + 2, NY)

    masters = [
        pltpu.make_async_copy(src, dst, ms.at[i])
        for i, (src, dst) in enumerate(((gm_hbm, gm_ref), (um_hbm, um_ref), (dm_hbm, dm_ref)))
    ]
    for m in masters:
        m.start()

    barrier = pltpu.get_barrier_semaphore()
    count = 0
    for dy in range(NY):
        for dt in range(NT):
            if dy or dt:
                pl.semaphore_signal(barrier, inc=1, device_id=at(g, z, rem(y + dy, NY), rem(t + dt, NT)), device_id_type=MESH)
                count += 1
    for dg in range(2):
        for dz in range(NZ):
            if dg or dz:
                pl.semaphore_signal(barrier, inc=1, device_id=at(rem(g + dg, 2), rem(z + dz, NZ), y, t), device_id_type=MESH)
                count += 1

    ex = lax.broadcasted_iota(I32, (16, TOK), 0)
    first_is, second_is = routes_ref[0:1, :] == ex, routes_ref[1:2, :] == ex
    named = first_is | second_is
    before = lax.broadcasted_iota(I32, (TOK, TOK), 0) < lax.broadcasted_iota(I32, (TOK, TOK), 1)
    rank = jnp.dot(
        jnp.where(named, 1.0, 0.0).astype(BF), jnp.where(before, 1.0, 0.0).astype(BF), preferred_element_type=F32
    )
    key_ref[...] = jnp.where(named, rank, -1.0)
    mix_ref[...] = jnp.where(first_is, weight_ref[0:1, :], 0.0) + jnp.where(second_is, weight_ref[1:2, :], 0.0)
    slot = lax.broadcasted_iota(I32, (CAP, TOK), 0).astype(F32)

    def tables(k, _):
        key = key_ref[pl.ds(rem(t + k, NT), 1), :]
        table_ref[k] = jnp.where(slot == key, 1.0, 0.0).astype(BF)
        return 0

    lax.fori_loop(0, NT, tables, 0)
    t_ref[z] = tok_ref[...]

    pl.semaphore_wait(barrier, count)

    low, base = rem(z, 2), 2 * lax.div(z, 2)
    peers = {1: base + 1 - low, 2: 2 - base + low, 3: 3 - base - low}

    def tok_copy(i):
        return send(tok_ref, t_ref.at[z], zs.at[i], zr.at[i], at(g, peers[i], y, t))

    for i in (1, 2, 3):
        tok_copy(i).start()

    def first(k, h):
        return send(
            wp_ref.at[k, h], q_ref.at[x, y], qs.at[k, h], qr.at[x * NY + y],
            at(g, z, NC * c + h, rem(t + k, NT)),
        )

    def first_start(k):
        for h in range(2):
            mine = (NC * c + h == y) & (rem(t + k, NT) == t)

            @pl.when(mine)
            def _():
                pltpu.make_async_copy(wp_ref.at[k, h], q_ref.at[x, y], qr.at[x * NY + y]).start()

            @pl.when(jnp.logical_not(mine))
            def _():
                first(k, h).start()

    for m in masters:
        m.wait()
    gain = jnp.concatenate([gain_ref[...], gain_ref[...]], axis=1)

    def pack(i, _):
        k = 4 + (1 - 2 * rem(i, 2)) * lax.div(i + 1, 2)
        e = rem(t + k, NT)
        pad = jnp.zeros((2 * ROWS, 3 * LANES - WIDTH), F32)
        gu = jnp.concatenate([gm_ref[e], um_ref[e]], axis=0)
        gu = (jnp.transpose(jnp.concatenate([gu, pad], axis=1)) * gain).astype(BF)
        dn = dm_ref[e]
        dn = jnp.concatenate([dn, pad[:ROWS]], axis=1)
        dd = jnp.concatenate([dn, pltpu.roll(dn, 3 * LANES - DLO, 1)], axis=0)
        dd = jnp.transpose(dd).astype(BF)
        for h in range(2):
            lo = h * COLS
            wp_ref[k, h, 0:COLS, :] = gu[lo:lo + COLS]
            wp_ref[k, h, COLS:PACK, :] = dd[lo:lo + DLO]

        @pl.when(i > 0)
        def _():
            j = i - 1
            first_start(4 + (1 - 2 * rem(j, 2)) * lax.div(j + 1, 2))

        return 0

    lax.fori_loop(0, NT, pack, 0)
    first_start(0)

    def pair_of(q):
        return lax.div(z, 2) if q == 0 else 1 - lax.div(z, 2)

    def dispatch(q):
        lo = 2 * pair_of(q)
        rows_in = jnp.concatenate([t_ref[lo], t_ref[lo + 1]], axis=1)
        for k in NEAR:
            rows = jnp.dot(table_ref[k], rows_in, preferred_element_type=F32).astype(BF)
            if k:
                s_ref[q, k] = rows
            else:
                x_ref[pair_of(q), t, y] = rows

    def across(q, k):
        return send(s_ref.at[q, k], x_ref.at[pair_of(q), t, y], xs.at[q, k], xr.at[q, k], at(g, z, y, rem(t + k, NT)))

    def along(q, k, way):
        b = rem(t + NT - k, NT)
        whose = y if way < 2 else (dn_y if k % 2 == 0 else up_y)
        to = up_y if way == 0 or (way == 2 and k % 2 == 0) else dn_y
        ref = x_ref.at[pair_of(q), b, whose]
        return send(ref, ref, ys.at[q, k, way], yr.at[q, k, way], at(g, z, to, t))

    def spread(q, k):
        if k:
            across(q, k).wait_recv()
        along(q, k, 0).start()
        along(q, k, 1).start()

    def forward(q, k):
        along(q, k, k % 2).wait_recv()
        along(q, k, 2).start()

    zz = g * NZ + z

    def second(j, q):
        zd = rem(z + j, NZ)
        return send(q_ref.at[zd], v_ref.at[zz], vs.at[j, q], vr.at[j, q], at(rem(g + q, 2), zd, y, t))

    own_v = pltpu.make_async_copy(q_ref.at[z], v_ref.at[zz], vr.at[0, 0])

    def weights_on(j):
        zd = rem(z + j, NZ)
        for i in range(NY):
            send(q_ref.at[zd, i], q_ref.at[zd, i], qs.at[0, 0], qr.at[zd * NY + i], at(g, z, up_y, t)).wait_recv()
        for q in (1, 0):
            if j or q:
                second(j, q).start()
            else:
                own_v.start()

    tok_copy(1).wait_recv()
    dispatch(0)
    for k in NEAR[1:]:
        across(0, k).start()
    spread(0, 0)
    spread(0, 1)
    tok_copy(2).wait_recv()
    tok_copy(3).wait_recv()
    dispatch(1)
    for k in NEAR[1:]:
        across(1, k).start()
    spread(1, 0)
    spread(0, 7)
    for j in (2, 1, 3, 0):
        weights_on(j)
        spread(0, NEAR[3 + (2, 1, 3, 0).index(j)])
    spread(0, NEAR[7])
    for k in NEAR:
        forward(0, k)
        if k:
            spread(1, k)
    for k in NEAR:
        forward(1, k)

    def weighting(k, _):
        e = rem(t + NT - k, NT)
        here = slot == key_ref[pl.ds(e, 1), :]
        mix = mix_ref[pl.ds(e, 1), :]
        high = mix.astype(BF).astype(F32)
        for i, part in enumerate((high, mix - high)):
            comb_ref[k, i] = jnp.transpose(jnp.where(here, part, 0.0)).astype(BF)
        return 0

    lax.fori_loop(0, NT, weighting, 0)

    left = lax.broadcasted_iota(I32, (COLS, LANES), 1) < ROWS

    def unpack(zs_):
        for i in range(NY // 2):
            a, b = (v_ref[zs_, 2 * i + n].astype(F32) for n in range(2))
            ra, rb = pltpu.roll(a, ROWS, 1), pltpu.roll(b, ROWS, 1)
            cols = pl.ds(pl.multiple_of((zs_ * (NY // 2) + i) * LANES, LANES), LANES)
            gate_ref[:, cols] = jnp.where(left, a[:COLS], rb[:COLS]).astype(BF)
            up_ref[:, cols] = jnp.where(left, ra[:COLS], b[:COLS]).astype(BF)
            down_ref[0:DLO, cols] = jnp.where(left[:DLO], a[COLS:], rb[COLS:]).astype(BF)
            down_ref[DLO:COLS, cols] = jnp.where(left[:DHI], ra[COLS:COLS + DHI], b[COLS:COLS + DHI]).astype(BF)

    own_v.wait()
    unpack(zz)
    for j, q in ((1, 0), (3, 0), (2, 0), (1, 1), (3, 1), (2, 1), (0, 1)):
        second(j, q).wait_recv()
        unpack(rem(g + q, 2) * NZ + rem(z + NZ - j, NZ))
    served = [
        pltpu.make_async_copy(src, dst.at[0], outs.at[i])
        for i, (src, dst) in enumerate(((gate_ref, gate_out), (up_ref, up_out), (down_ref, down_out)))
    ]
    for m in served:
        m.start()

    for q in range(2):
        for k in NEAR:
            along(q, k, 1 - k % 2).wait_recv()
            along(q, k, 2).wait_recv()

    def near(k):
        return rem(y + 1 + 2 * rem(k, 2), NY)

    def other(k):
        return rem(y + 3 - 2 * rem(k, 2), NY)

    def far(n, k):
        return send(p_ref.at[n, k, far_y], r_ref.at[n, k], fs.at[n, k], fr.at[n, k], at(g, z, near(k), t))

    def plain(n, k):
        return send(p_ref.at[n, k, other(k)], u_ref.at[n, k], us.at[n, k], ur.at[n, k], at(g, z, other(k), t))

    def summed(n, k):
        return send(a_ref.at[n, k], w_ref.at[n, k], ws.at[n, k], wr.at[n, k], at(g, z, near(k), t))

    def back(n, k):
        return send(o_ref.at[n, k], e_ref.at[n, k], bs.at[n, k], br.at[n, k], at(g, z, y, rem(t + k, NT)))

    def experts(k):
        b = rem(t + k, NT)
        rows = jnp.concatenate(
            [x_ref[zi // 2, b, yi, :, (zi % 2) * FEAT:(zi % 2 + 1) * FEAT] for zi in range(NZ) for yi in range(NY)],
            axis=1,
        )
        wide = rows.astype(F32)
        scale = lax.rsqrt(jnp.sum(wide * wide, axis=1, keepdims=True) / MODEL + norm_eps)
        rows = (wide * scale).astype(BF)
        dims = (((1,), (1,)), ((), ()))
        gate = lax.dot_general(rows, gate_ref[...], dims, preferred_element_type=F32)
        up = lax.dot_general(rows, up_ref[...], dims, preferred_element_type=F32)
        h_ref[k] = (gate / (1.0 + jnp.exp(-gate)) * up).astype(BF)

    def products(n, k):
        hidden = h_ref[k]
        for i, zi in enumerate(HALVES[n]):
            part = jnp.dot(hidden, down_ref[:, zi * NY * FEAT:(zi + 1) * NY * FEAT], preferred_element_type=F32).astype(BF)
            for yi in range(NY):
                p_ref[n, k, yi, :, i * FEAT:(i + 1) * FEAT] = part[:, yi * FEAT:(yi + 1) * FEAT]

    def kth(i):
        return 4 + (1 - 2 * rem(i, 2)) * lax.div(i + 1, 2)

    def sweep0(i, _):
        k = kth(i)
        experts(k)
        products(0, k)
        far(0, k).start()
        plain(0, k).start()
        return 0

    def relay(n, k):
        far(n, k).wait_recv()
        a_ref[n, k] = (r_ref[n, k].astype(F32) + p_ref[n, k, near(k)].astype(F32)).astype(BF)
        summed(n, k).start()

    def finish(n, k):
        plain(n, k).wait_recv()
        summed(n, k).wait_recv()
        total = (p_ref[n, k, y].astype(F32) + u_ref[n, k].astype(F32) + w_ref[n, k].astype(F32)).astype(BF)

        @pl.when(k > 0)
        def _():
            o_ref[n, k] = total
            back(n, k).start()

        @pl.when(k == 0)
        def _():
            e_ref[n, k] = total

    def sweep1(i, _):
        k = kth(i)
        relay(0, k)
        products(1, k)
        far(1, k).start()
        plain(1, k).start()
        return 0

    def sweep2(i, _):
        k = kth(i)
        relay(1, k)
        finish(0, k)
        return 0

    def sweep3(i, _):
        finish(1, kth(i))
        return 0

    lax.fori_loop(0, NT, sweep0, 0)
    lax.fori_loop(0, NT, sweep1, 0)
    lax.fori_loop(0, NT, sweep2, 0)

    def combine(n):
        total = jnp.zeros((TOK, 2 * FEAT), F32)
        for k in FARS:
            if k:
                back(n, k).wait_recv()
            for i in range(2):
                total = total + jnp.dot(comb_ref[k, i], e_ref[n, k], preferred_element_type=F32)
        for i, zi in enumerate(HALVES[n]):
            m_ref[zi] = total[:, i * FEAT:(i + 1) * FEAT].astype(BF)

    def part(zi, zo):
        return send(m_ref.at[zo], l_ref.at[zi], cs.at[zo], cr.at[zi], at(g, zo, y, t))

    def home(n):
        for zo in HALVES[n]:
            @pl.when(zo != z)
            def _():
                part(z, zo).start()

    combine(0)
    home(0)
    lax.fori_loop(0, NT, sweep3, 0)
    combine(1)
    home(1)

    l_ref[z] = m_ref[z]
    own = jnp.zeros((TOK, FEAT), F32)
    for zi in range(NZ):
        @pl.when(zi != z)
        def _():
            part(zi, z).wait_recv()
    for zi in range(NZ):
        own = own + l_ref[zi].astype(F32)
    out_ref[...] = own.astype(BF)

    for m in served:
        m.wait()
    for i in (1, 2, 3):
        tok_copy(i).wait_send()
    for k in range(NT):
        for h in range(2):
            if k:
                first(k, h).wait_send()
            else:
                @pl.when(NC * c + h != y)
                def _():
                    first(k, h).wait_send()
    for j in range(NZ):
        for q in range(2):
            if j or q:
                second(j, q).wait_send()
    for n in range(2):
        for k in range(NT):
            for way in range(3):
                along(n, k, way).wait_send()
            if k:
                across(n, k).wait_send()
                back(n, k).wait_send()
            far(n, k).wait_send()
            plain(n, k).wait_send()
            summed(n, k).wait_send()
    for zo in range(NZ):
        @pl.when(zo != z)
        def _():
            part(z, zo).wait_send()


def local(tokens, routes, route_weight, norm_gain, gate_master, up_master, down_master):
    vm = pl.BlockSpec(memory_space=pltpu.VMEM)
    any_ = pl.BlockSpec(memory_space=pl.ANY)
    dma = pltpu.SemaphoreType.DMA
    serving = jax.ShapeDtypeStruct((1, COLS, MODEL), BF)
    master = pltpu.VMEM((EXPERTS, ROWS, WIDTH), F32)
    half = pltpu.VMEM((2, NT, CAP, 2 * FEAT), BF)
    mixed, gate_t, up_t, down_t = pl.pallas_call(
        kernel,
        out_shape=(jax.ShapeDtypeStruct((TOK, FEAT), BF), serving, serving, serving),
        in_specs=[vm, vm, vm, vm, any_, any_, any_],
        out_specs=(vm, any_, any_, any_),
        scratch_shapes=[
            master, master, master,
            pltpu.VMEM((16, TOK), F32),
            pltpu.VMEM((16, TOK), F32),
            pltpu.VMEM((NT, CAP, TOK), BF),
            pltpu.VMEM((NT, 2, TOK, CAP), BF),
            pltpu.VMEM((NT, 2, PACK, LANES), BF),
            pltpu.VMEM((NX, NY, PACK, LANES), BF),
            pltpu.VMEM((2 * NZ, NY, PACK, LANES), BF),
            pltpu.VMEM((NZ, TOK, FEAT), BF),
            half,
            pltpu.VMEM((2, NT, NY, CAP, 2 * FEAT), BF),
            pltpu.VMEM((COLS, MODEL), BF),
            pltpu.VMEM((COLS, MODEL), BF),
            pltpu.VMEM((COLS, MODEL), BF),
            pltpu.VMEM((NT, CAP, COLS), BF),
            pltpu.VMEM((2, NT, NY, CAP, 2 * FEAT), BF),
            half, half, half, half, half, half,
            pltpu.VMEM((NZ, TOK, FEAT), BF),
            pltpu.VMEM((NZ, TOK, FEAT), BF),
            dma((3,)), dma((NZ,)), dma((NZ,)),
            dma((NT, 2)), dma((NX * NY,)),
            dma((NZ, 2)), dma((NZ, 2)),
            dma((2, NT)), dma((2, NT)),
            dma((2, NT, 3)), dma((2, NT, 3)),
            dma((2, NT)), dma((2, NT)), dma((2, NT)), dma((2, NT)),
            dma((2, NT)), dma((2, NT)), dma((2, NT)), dma((2, NT)),
            dma((NZ,)), dma((NZ,)), dma((3,)),
        ],
        compiler_params=pltpu.CompilerParams(collective_id=0, has_side_effects=True, vmem_limit_bytes=VMEM_LIMIT),
        name="handover_kernel",
    )(tokens, routes.T, route_weight.T, norm_gain[None, :], gate_master, up_master, down_master)
    return mixed, jnp.swapaxes(gate_t, 1, 2), jnp.swapaxes(up_t, 1, 2), jnp.swapaxes(down_t, 1, 2)


def solution(mesh):
    placed = (
        P(("gr", "tp"), "fs"),
        P(("gr", "tp"), None),
        P(("gr", "tp"), None),
        P(("gr", "fs")),
        P(None, ("gr", "fs"), "tp"),
        P(None, ("gr", "fs"), "tp"),
        P(None, ("gr", "fs"), "tp"),
    )
    return jax.shard_map(
        local,
        mesh=mesh,
        in_specs=placed,
        out_specs=(
            P(("gr", "tp"), "fs"),
            P("tp", None, "fs"),
            P("tp", None, "fs"),
            P("tp", None, "fs"),
        ),
        check_vma=False,
    )
```

time: 407 us -> 155 us (0.38); the launches traced: 402 us -> 155 us
  waiting for transfers between devices: 161 us -> 0 us
  Pallas kernels: 0 us -> 148 us
  blocking collectives: 142 us -> 0 us
  local copies, waits for them, and re-layouts: 45.2 us -> 5.91 us
  matrix products: 18.1 us -> 0 us
  between operations: 14.4 us -> 0.64 us
  starting transfers between devices: 12.5 us -> 0 us
  other arithmetic: 8.05 us -> 0 us
    reduce_scatter x1 -> x0, waiting for transfers between devices: 151 us -> none  [local(): lax.psum_scatter(partial_value, 'fs', scatter_dimension=3, tiled=True)]
    pallas_call x0 -> x1, Pallas kernels: none -> 148 us  [local(): pl.pallas_call(kernel, out_shape=(jax.ShapeDtypeStruct((TOK, FEAT), BF),...]
    all_to_all x4 -> x0, blocking collectives: 142 us -> none  [the longest x2 72.2 us: sent_together(): lax.all_to_all(both, axis, split_axis=split_dim, concat_axis=concat_dim,...]
    dot_general x3 -> x0, matrix products: 18.1 us -> none  [the longest x1 11.5 us: local(): jnp.einsum('sjcf,jdf->sjcd', hidden, down_w, preferred_element_type=jnp.f...]
    all_to_all x2 -> x0, starting transfers between devices: 12.5 us -> none  [the longest x1 8.2 us: copy_for_each(): lax.all_to_all(jnp.broadcast_to(shard[None], (devices, *shard.shape)), ax...]
    split x11 -> x0, local copies, waits for them, and re-layouts: 10.7 us -> none  [the longest x6 8.66 us: sent_together_2(): jnp.split(out, [sum(widths[:k]) for k in range(1, len(widths))], axis=along)]
    all_to_all x2 -> x0, waiting for transfers between devices: 10.3 us -> none  [the longest x1 10.3 us: local(): lax.all_to_all(summed, 'tp', split_axis=0, concat_axis=0, tiled=True)]
    another operation x3 -> x0, local copies, waits for them, and re-layouts: 9.23 us -> none
  transfers between devices with their start and end apart: 4 -> 0, of which waited for: 2 -> 0; matrix products, arithmetic and copies ran while one was open for 12% -> 0% of each run, Pallas kernels for 0% -> 0%
where the time goes in v2:
time: 155 us
  Pallas kernels  148 us (95%)
  local copies, waits for them, and re-layouts  5.91 us (4%)
    pallas_call x1, Pallas kernels, local(): pl.pallas_call(kernel, out_shape=(jax.ShapeDtypeStruct((TOK, FEAT), BF),...  148 us
    unnamed x8, local copies, waits for them, and re-layouts  5.91 us

profile of v2, /device:TPU:64, one launch (start us, length us, event | category | flops | bytes accessed | tf_op | source)
XLA Modules:
  0.0 155.0 jit_solution(7294168143625906572)
XLA Ops:
  0.6 148.5 %handover_kernel.1 = (bf16[512,128]{1,0:T(8,128)(2,1)}, bf16[1,176,2048]{2,1,0:T(8,128)(2,1)}, bf16[1,176,2048]{2,1,0:T(8,128)(2,1)}, bf16[1,176,2048]{2,1,0:T(8,128)(2,1)}) custom-call(bf16[512,128]{1,0:T(8,128)(2,1)} %tok_ref.1, s32[2,512]{1,0:T(2,128)} %bitcast.9, f32[2,512]{1,0:T(2,128)} %bitcast.10, f32[1,64]{1,0:T(1,128)} %bitcast.11, ...), custom_call_target="tpu_custom_call" | custom-call | tf_op jit(solution)/shard_map/handover_kernel/pallas_call | solution.py:438
  149.1 1.6 %copy.15 = bf16[512,128]{1,0:T(8,128)(2,1)} copy(bf16[512,128]{1,0:T(8,128)(2,1)} %get-tuple-element.16) | data formatting | bytes 262144
  150.7 0.0 copy-start.1
  150.7 2.1 %copy.16 = bf16[1,2048,176]{1,2,0:T(8,128)(2,1)} copy(bf16[1,2048,176]{1,2,0:T(8,128)(2,1)} %bitcast.8) | data formatting | bytes 1441792
  152.8 0.0 copy-done.1
  152.8 0.0 copy-start
  152.8 0.9 copy.17
  153.7 0.5 copy-done
  154.2 0.9 copy.18
Async XLA Ops:
  150.7 2.1 %copy-start.1 = (bf16[1,176,2048]{2,1,0:T(8,128)(2,1)S(1)}, bf16[1,176,2048]{2,1,0:T(8,128)(2,1)}, u32[]{:S(2)}) copy-start(bf16[1,176,2048]{2,1,0:T(8,128)(2,1)} %get-tuple-element.10) | copy-start | bytes 2162692
  152.8 1.4 copy-start

commit v3 on v2

--- a/solution.py
+++ b/solution.py
@@ -27,7 +27,8 @@
 MODEL = 2048
 NEAR = (0, 1, 7, 2, 6, 3, 5, 4)
 FARS = (4, 3, 5, 2, 6, 1, 7, 0)
-HALVES = ((0, 3), (1, 2))
+PARTS = ((0, 3), (2,))
+LATE = 1
 
 
 def rem(a, n):
@@ -48,11 +49,12 @@
     tok_ref, routes_ref, weight_ref, gain_ref, gm_hbm, um_hbm, dm_hbm,
     out_ref, gate_out, up_out, down_out,
     gm_ref, um_ref, dm_ref, key_ref, mix_ref, table_ref, comb_ref,
-    wp_ref, q_ref, v_ref, t_ref, s_ref, x_ref, gate_ref, up_ref, down_ref, h_ref,
-    p_ref, r_ref, a_ref, u_ref, w_ref, o_ref, e_ref, m_ref, l_ref,
-    ms, zs, zr, qs, qr, vs, vr, xs, xr, ys, yr,
-    fs, fr, us, ur, ws, wr, bs, br, cs, cr, outs,
+    wp_ref, q_ref, v_ref, t_ref, ty_ref, s0_ref, s1_ref, s2_ref, x_ref, gate_ref, up_ref, down_ref, h_ref,
+    p0, r0, a0, u0, w0, o0, e0, p1, r1, a1, u1, w1, o1, e1, pl_ref, el_ref, my_ref, ly_ref, m_ref, l_ref,
+    ms, zs, zr, tys, tyr, qs, qr, vs, vr, xs, xr, ys, yr,
+    fs, fr, us, ur, ws, wr, bs, br, ds, dr, cs, cr, outs,
 ):
+    ps, rs_, as_, us_, ws_, os_, es = ((p0, p1), (r0, r1), (a0, a1), (u0, u1), (w0, w1), (o0, o1), (e0, e1))
     g, f, t = lax.axis_index("gr"), lax.axis_index("fs"), lax.axis_index("tp")
     z, y = lax.div(f, NY), rem(f, NY)
     x, c = lax.div(t, NC), rem(t, NC)
@@ -95,7 +97,7 @@
         return 0
 
     lax.fori_loop(0, NT, tables, 0)
-    t_ref[z] = tok_ref[...]
+    ty_ref[y] = tok_ref[...]
 
     pl.semaphore_wait(barrier, count)
 
@@ -105,8 +107,13 @@
     def tok_copy(i):
         return send(tok_ref, t_ref.at[z], zs.at[i], zr.at[i], at(g, peers[i], y, t))
 
+    def tok_along(i):
+        return send(tok_ref, ty_ref.at[y], tys.at[i], tyr.at[i], at(g, z, rem(y + i, NY), t))
+
     for i in (1, 2, 3):
         tok_copy(i).start()
+    for i in (1, 3, 2):
+        tok_along(i).start()
 
     def first(k, h):
         return send(
@@ -155,27 +162,46 @@
     lax.fori_loop(0, NT, pack, 0)
     first_start(0)
 
-    def pair_of(q):
-        return lax.div(z, 2) if q == 0 else 1 - lax.div(z, 2)
+    mate, rest = peers[1], 2 - base
+    tiles = (mate, pl.ds(rest, 2))
+    stage = (s0_ref, s1_ref)
 
     def dispatch(q):
-        lo = 2 * pair_of(q)
-        rows_in = jnp.concatenate([t_ref[lo], t_ref[lo + 1]], axis=1)
+        rows_in = t_ref[mate] if q == 0 else jnp.concatenate([t_ref[rest], t_ref[rest + 1]], axis=1)
         for k in NEAR:
             rows = jnp.dot(table_ref[k], rows_in, preferred_element_type=F32).astype(BF)
-            if k:
-                s_ref[q, k] = rows
-            else:
-                x_ref[pair_of(q), t, y] = rows
+            for i in range(1 + q):
+                part = rows[:, i * FEAT:(i + 1) * FEAT]
+                if k == 0:
+                    x_ref[rest + i if q else mate, t, y] = part
+                elif q:
+                    s1_ref[k, i] = part
+                else:
+                    s0_ref[k] = part
+
+    def dispatch_own():
+        rows_in = jnp.concatenate([ty_ref[i] for i in range(NY)], axis=1)
+        for k in NEAR:
+            rows = jnp.dot(table_ref[k], rows_in, preferred_element_type=F32).astype(BF)
+            for i in range(NY):
+                part = rows[:, i * FEAT:(i + 1) * FEAT]
+                if k == 0:
+                    x_ref[z, t, i] = part
+                else:
+                    s2_ref[k, i] = part
 
     def across(q, k):
-        return send(s_ref.at[q, k], x_ref.at[pair_of(q), t, y], xs.at[q, k], xr.at[q, k], at(g, z, y, rem(t + k, NT)))
+        if q == 2:
+            src, dst = s2_ref.at[k], x_ref.at[z, t]
+        else:
+            src, dst = stage[q].at[k], x_ref.at[tiles[q], t, y]
+        return send(src, dst, xs.at[q, k], xr.at[q, k], at(g, z, y, rem(t + k, NT)))
 
     def along(q, k, way):
         b = rem(t + NT - k, NT)
         whose = y if way < 2 else (dn_y if k % 2 == 0 else up_y)
         to = up_y if way == 0 or (way == 2 and k % 2 == 0) else dn_y
-        ref = x_ref.at[pair_of(q), b, whose]
+        ref = x_ref.at[tiles[q], b, whose]
         return send(ref, ref, ys.at[q, k, way], yr.at[q, k, way], at(g, z, to, t))
 
     def spread(q, k):
@@ -211,18 +237,21 @@
     for k in NEAR[1:]:
         across(0, k).start()
     spread(0, 0)
-    spread(0, 1)
     tok_copy(2).wait_recv()
     tok_copy(3).wait_recv()
     dispatch(1)
     for k in NEAR[1:]:
         across(1, k).start()
     spread(1, 0)
-    spread(0, 7)
+    for i in (1, 3, 2):
+        tok_along(i).wait_recv()
+    dispatch_own()
+    for k in FARS[:-1]:
+        across(2, k).start()
     for j in (2, 1, 3, 0):
         weights_on(j)
-        spread(0, NEAR[3 + (2, 1, 3, 0).index(j)])
-    spread(0, NEAR[7])
+    for k in NEAR[1:]:
+        spread(0, k)
     for k in NEAR:
         forward(0, k)
         if k:
@@ -269,6 +298,8 @@
         for k in NEAR:
             along(q, k, 1 - k % 2).wait_recv()
             along(q, k, 2).wait_recv()
+    for k in FARS[:-1]:
+        across(2, k).wait_recv()
 
     def near(k):
         return rem(y + 1 + 2 * rem(k, 2), NY)
@@ -277,21 +308,22 @@
         return rem(y + 3 - 2 * rem(k, 2), NY)
 
     def far(n, k):
-        return send(p_ref.at[n, k, far_y], r_ref.at[n, k], fs.at[n, k], fr.at[n, k], at(g, z, near(k), t))
+        return send(ps[n].at[k, far_y], rs_[n].at[k], fs.at[n, k], fr.at[n, k], at(g, z, near(k), t))
 
     def plain(n, k):
-        return send(p_ref.at[n, k, other(k)], u_ref.at[n, k], us.at[n, k], ur.at[n, k], at(g, z, other(k), t))
+        return send(ps[n].at[k, other(k)], us_[n].at[k], us.at[n, k], ur.at[n, k], at(g, z, other(k), t))
 
     def summed(n, k):
-        return send(a_ref.at[n, k], w_ref.at[n, k], ws.at[n, k], wr.at[n, k], at(g, z, near(k), t))
+        return send(as_[n].at[k], ws_[n].at[k], ws.at[n, k], wr.at[n, k], at(g, z, near(k), t))
 
     def back(n, k):
-        return send(o_ref.at[n, k], e_ref.at[n, k], bs.at[n, k], br.at[n, k], at(g, z, y, rem(t + k, NT)))
+        src, dst = (os_[n].at[k], es[n].at[k]) if n < 2 else (pl_ref.at[k], el_ref.at[k])
+        return send(src, dst, bs.at[n, k], br.at[n, k], at(g, z, y, rem(t + k, NT)))
 
     def experts(k):
         b = rem(t + k, NT)
         rows = jnp.concatenate(
-            [x_ref[zi // 2, b, yi, :, (zi % 2) * FEAT:(zi % 2 + 1) * FEAT] for zi in range(NZ) for yi in range(NY)],
+            [x_ref[zi, b, yi] for zi in range(NZ) for yi in range(NY)],
             axis=1,
         )
         wide = rows.astype(F32)
@@ -302,12 +334,15 @@
         up = lax.dot_general(rows, up_ref[...], dims, preferred_element_type=F32)
         h_ref[k] = (gate / (1.0 + jnp.exp(-gate)) * up).astype(BF)
 
+    def product(zi, k):
+        cols = slice(zi * NY * FEAT, (zi + 1) * NY * FEAT)
+        return jnp.dot(h_ref[k], down_ref[:, cols], preferred_element_type=F32).astype(BF)
+
     def products(n, k):
-        hidden = h_ref[k]
-        for i, zi in enumerate(HALVES[n]):
-            part = jnp.dot(hidden, down_ref[:, zi * NY * FEAT:(zi + 1) * NY * FEAT], preferred_element_type=F32).astype(BF)
+        for i, zi in enumerate(PARTS[n]):
+            part = product(zi, k)
             for yi in range(NY):
-                p_ref[n, k, yi, :, i * FEAT:(i + 1) * FEAT] = part[:, yi * FEAT:(yi + 1) * FEAT]
+                ps[n][k, yi, :, i * FEAT:(i + 1) * FEAT] = part[:, yi * FEAT:(yi + 1) * FEAT]
 
     def kth(i):
         return 4 + (1 - 2 * rem(i, 2)) * lax.div(i + 1, 2)
@@ -316,28 +351,39 @@
         k = kth(i)
         experts(k)
         products(0, k)
+        late = product(LATE, k)
         far(0, k).start()
         plain(0, k).start()
+
+        @pl.when(k > 0)
+        def _():
+            pl_ref[k] = late
+            back(2, k).start()
+
+        @pl.when(k == 0)
+        def _():
+            el_ref[k] = late
+
         return 0
 
     def relay(n, k):
         far(n, k).wait_recv()
-        a_ref[n, k] = (r_ref[n, k].astype(F32) + p_ref[n, k, near(k)].astype(F32)).astype(BF)
+        as_[n][k] = (rs_[n][k].astype(F32) + ps[n][k, near(k)].astype(F32)).astype(BF)
         summed(n, k).start()
 
     def finish(n, k):
         plain(n, k).wait_recv()
         summed(n, k).wait_recv()
-        total = (p_ref[n, k, y].astype(F32) + u_ref[n, k].astype(F32) + w_ref[n, k].astype(F32)).astype(BF)
+        total = (ps[n][k, y].astype(F32) + us_[n][k].astype(F32) + ws_[n][k].astype(F32)).astype(BF)
 
         @pl.when(k > 0)
         def _():
-            o_ref[n, k] = total
+            os_[n][k] = total
             back(n, k).start()
 
         @pl.when(k == 0)
         def _():
-            e_ref[n, k] = total
+            es[n][k] = total
 
     def sweep1(i, _):
         k = kth(i)
@@ -357,34 +403,54 @@
         finish(1, kth(i))
         return 0
 
-    lax.fori_loop(0, NT, sweep0, 0)
-    lax.fori_loop(0, NT, sweep1, 0)
-    lax.fori_loop(0, NT, sweep2, 0)
-
-    def combine(n):
-        total = jnp.zeros((TOK, 2 * FEAT), F32)
+    def combined(n):
+        rows = es[n] if n < 2 else el_ref
+        total = jnp.zeros((TOK, rows.shape[-1]), F32)
         for k in FARS:
             if k:
                 back(n, k).wait_recv()
             for i in range(2):
-                total = total + jnp.dot(comb_ref[k, i], e_ref[n, k], preferred_element_type=F32)
-        for i, zi in enumerate(HALVES[n]):
-            m_ref[zi] = total[:, i * FEAT:(i + 1) * FEAT].astype(BF)
+                total = total + jnp.dot(comb_ref[k, i], rows[k], preferred_element_type=F32)
+        return total
+
+    def token_sum(i):
+        to = rem(y + i, NY)
+        return send(my_ref.at[to], ly_ref.at[y], ds.at[i], dr.at[i], at(g, z, to, t))
 
     def part(zi, zo):
         return send(m_ref.at[zo], l_ref.at[zi], cs.at[zo], cr.at[zi], at(g, zo, y, t))
 
-    def home(n):
-        for zo in HALVES[n]:
-            @pl.when(zo != z)
-            def _():
-                part(z, zo).start()
-
+    def home(zo):
+        @pl.when(zo != z)
+        def _():
+            part(z, zo).start()
+
+    def combine(n):
+        total = combined(n)
+        for i, zo in enumerate(PARTS[n]):
+            m_ref[zo] = total[:, i * FEAT:(i + 1) * FEAT].astype(BF)
+        for zo in PARTS[n]:
+            home(zo)
+
+    lax.fori_loop(0, NT, sweep0, 0)
+    lax.fori_loop(0, NT, sweep1, 0)
+    total = combined(2)
+    for i in range(NY):
+        my_ref[i] = total[:, i * FEAT:(i + 1) * FEAT].astype(BF)
+    for i in (1, 3, 2):
+        token_sum(i).start()
+    lax.fori_loop(0, NT, sweep2, 0)
     combine(0)
-    home(0)
+    ly_ref[y] = my_ref[y]
+    for i in (1, 3, 2):
+        token_sum(i).wait_recv()
+    total = jnp.zeros((TOK, FEAT), F32)
+    for i in range(NY):
+        total = total + ly_ref[i].astype(F32)
+    m_ref[LATE] = total.astype(BF)
+    home(LATE)
     lax.fori_loop(0, NT, sweep3, 0)
     combine(1)
-    home(1)
 
     l_ref[z] = m_ref[z]
     own = jnp.zeros((TOK, FEAT), F32)
@@ -400,6 +466,8 @@
         m.wait()
     for i in (1, 2, 3):
         tok_copy(i).wait_send()
+        tok_along(i).wait_send()
+        token_sum(i).wait_send()
     for k in range(NT):
         for h in range(2):
             if k:
@@ -412,6 +480,9 @@
         for q in range(2):
             if j or q:
                 second(j, q).wait_send()
+    for k in range(1, NT):
+        across(2, k).wait_send()
+        back(2, k).wait_send()
     for n in range(2):
         for k in range(NT):
             for way in range(3):
@@ -428,16 +499,37 @@
             part(z, zo).wait_send()
 
 
+def hand_over(*refs):
+    src, dst, held, ins, outs = refs[:4], refs[4:8], refs[8:12], refs[12], refs[13]
+    reads = [pltpu.make_async_copy(src[i], held[i], ins.at[i]) for i in range(4)]
+    writes = [pltpu.make_async_copy(held[i], dst[i], outs.at[i]) for i in range(4)]
+    for r in reads:
+        r.start()
+    for r, w in zip(reads, writes):
+        r.wait()
+        w.start()
+    for w in writes:
+        w.wait()
+
+
 def local(tokens, routes, route_weight, norm_gain, gate_master, up_master, down_master):
     vm = pl.BlockSpec(memory_space=pltpu.VMEM)
     any_ = pl.BlockSpec(memory_space=pl.ANY)
     dma = pltpu.SemaphoreType.DMA
     serving = jax.ShapeDtypeStruct((1, COLS, MODEL), BF)
+    mixed = jax.ShapeDtypeStruct((TOK, FEAT), BF)
     master = pltpu.VMEM((EXPERTS, ROWS, WIDTH), F32)
-    half = pltpu.VMEM((2, NT, CAP, 2 * FEAT), BF)
-    mixed, gate_t, up_t, down_t = pl.pallas_call(
+
+    def rows(*dims):
+        return pltpu.VMEM((*dims[:-1], CAP, dims[-1]), BF)
+
+    def summing(width):
+        return [rows(NT, NY, width)] + [rows(NT, width)] * 6
+
+    shapes = (mixed, serving, serving, serving)
+    results = pl.pallas_call(
         kernel,
-        out_shape=(jax.ShapeDtypeStruct((TOK, FEAT), BF), serving, serving, serving),
+        out_shape=shapes,
         in_specs=[vm, vm, vm, vm, any_, any_, any_],
         out_specs=(vm, any_, any_, any_),
         scratch_shapes=[
@@ -450,29 +542,41 @@
             pltpu.VMEM((NX, NY, PACK, LANES), BF),
             pltpu.VMEM((2 * NZ, NY, PACK, LANES), BF),
             pltpu.VMEM((NZ, TOK, FEAT), BF),
-            half,
-            pltpu.VMEM((2, NT, NY, CAP, 2 * FEAT), BF),
+            pltpu.VMEM((NY, TOK, FEAT), BF),
+            rows(NT, FEAT), rows(NT, 2, FEAT), rows(NT, NY, FEAT),
+            rows(NZ, NT, NY, FEAT),
             pltpu.VMEM((COLS, MODEL), BF),
             pltpu.VMEM((COLS, MODEL), BF),
             pltpu.VMEM((COLS, MODEL), BF),
-            pltpu.VMEM((NT, CAP, COLS), BF),
-            pltpu.VMEM((2, NT, NY, CAP, 2 * FEAT), BF),
-            half, half, half, half, half, half,
+            rows(NT, COLS),
+            *summing(2 * FEAT), *summing(FEAT),
+            rows(NT, NY * FEAT), rows(NT, NY * FEAT),
+            pltpu.VMEM((NY, TOK, FEAT), BF),
+            pltpu.VMEM((NY, TOK, FEAT), BF),
             pltpu.VMEM((NZ, TOK, FEAT), BF),
             pltpu.VMEM((NZ, TOK, FEAT), BF),
-            dma((3,)), dma((NZ,)), dma((NZ,)),
+            dma((3,)), dma((NZ,)), dma((NZ,)), dma((NY,)), dma((NY,)),
             dma((NT, 2)), dma((NX * NY,)),
             dma((NZ, 2)), dma((NZ, 2)),
-            dma((2, NT)), dma((2, NT)),
+            dma((3, NT)), dma((3, NT)),
             dma((2, NT, 3)), dma((2, NT, 3)),
             dma((2, NT)), dma((2, NT)), dma((2, NT)), dma((2, NT)),
-            dma((2, NT)), dma((2, NT)), dma((2, NT)), dma((2, NT)),
+            dma((2, NT)), dma((2, NT)), dma((3, NT)), dma((3, NT)),
+            dma((NY,)), dma((NY,)),
             dma((NZ,)), dma((NZ,)), dma((3,)),
         ],
         compiler_params=pltpu.CompilerParams(collective_id=0, has_side_effects=True, vmem_limit_bytes=VMEM_LIMIT),
         name="handover_kernel",
     )(tokens, routes.T, route_weight.T, norm_gain[None, :], gate_master, up_master, down_master)
-    return mixed, jnp.swapaxes(gate_t, 1, 2), jnp.swapaxes(up_t, 1, 2), jnp.swapaxes(down_t, 1, 2)
+    out, gate_t, up_t, down_t = pl.pallas_call(
+        hand_over,
+        out_shape=shapes,
+        in_specs=[any_] * 4,
+        out_specs=(any_,) * 4,
+        scratch_shapes=[pltpu.VMEM(v.shape, BF) for v in shapes] + [dma((4,)), dma((4,))],
+        name="output_kernel",
+    )(*results)
+    return out, jnp.swapaxes(gate_t, 1, 2), jnp.swapaxes(up_t, 1, 2), jnp.swapaxes(down_t, 1, 2)
 
 
 def solution(mesh):

time: 155 us -> 146 us (0.942)
  local copies, waits for them, and re-layouts: 5.91 us -> 0 us
  Pallas kernels: 148 us -> 145 us
    unnamed x8 -> x0, local copies, waits for them, and re-layouts: 5.91 us -> none
    pallas_call x1 -> x2, Pallas kernels: 148 us -> 145 us  [the longest x1 142 us: local(): pl.pallas_call(kernel, out_shape=shapes, in_specs=[vm, vm, vm, vm, any_,...]
where the time goes in v3:
time: 146 us
  Pallas kernels  145 us (99%)
    pallas_call x1, Pallas kernels, local(): pl.pallas_call(kernel, out_shape=shapes, in_specs=[vm, vm, vm, vm, any_,...  142 us

profile of v3, /device:TPU:64, one launch (start us, length us, event | category | flops | bytes accessed | tf_op | source)
XLA Modules:
  0.0 145.6 jit_solution(14866433001899168855)
XLA Ops:
  0.6 142.4 %handover_kernel.1 = (bf16[512,128]{1,0:T(8,128)(2,1)}, bf16[1,176,2048]{2,1,0:T(8,128)(2,1)}, bf16[1,176,2048]{2,1,0:T(8,128)(2,1)}, bf16[1,176,2048]{2,1,0:T(8,128)(2,1)}) custom-call(bf16[512,128]{1,0:T(8,128)(2,1)} %tok_ref.1, s32[2,512]{1,0:T(2,128)} %bitcast.6, f32[2,512]{1,0:T(2,128)} %bitcast.7, f32[1,64]{1,0:T(1,128)} %bitcast.8, ...), custom_call_target="tpu_custom_call" | custom-call | tf_op jit(solution)/shard_map/handover_kernel/pallas_call | solution.py:530
  143.0 2.6 %output_kernel.1 = (bf16[512,128]{1,0:T(8,128)(2,1)}, bf16[1,176,2048]{2,1,0:T(8,128)(2,1)}, bf16[1,176,2048]{2,1,0:T(8,128)(2,1)}, bf16[1,176,2048]{2,1,0:T(8,128)(2,1)}) custom-call(bf16[512,128]{1,0:T(8,128)(2,1)} %get-tuple-element.12.refs_0_, bf16[1,176,2048]{2,1,0:T(8,128)(2,1)} %get-tuple-element.13.refs_1_, ...), custom_call_target="tpu_custom_call" | custom-call | tf_op jit(solution)/shard_map/output_kernel/pallas_call | solution.py:571

commit v4 on v3

--- a/solution.py
+++ b/solution.py
@@ -99,39 +99,16 @@
     lax.fori_loop(0, NT, tables, 0)
     ty_ref[y] = tok_ref[...]
 
-    pl.semaphore_wait(barrier, count)
-
-    low, base = rem(z, 2), 2 * lax.div(z, 2)
-    peers = {1: base + 1 - low, 2: 2 - base + low, 3: 3 - base - low}
-
-    def tok_copy(i):
-        return send(tok_ref, t_ref.at[z], zs.at[i], zr.at[i], at(g, peers[i], y, t))
-
-    def tok_along(i):
-        return send(tok_ref, ty_ref.at[y], tys.at[i], tyr.at[i], at(g, z, rem(y + i, NY), t))
-
-    for i in (1, 2, 3):
-        tok_copy(i).start()
-    for i in (1, 3, 2):
-        tok_along(i).start()
-
-    def first(k, h):
-        return send(
-            wp_ref.at[k, h], q_ref.at[x, y], qs.at[k, h], qr.at[x * NY + y],
-            at(g, z, NC * c + h, rem(t + k, NT)),
-        )
-
-    def first_start(k):
-        for h in range(2):
-            mine = (NC * c + h == y) & (rem(t + k, NT) == t)
-
-            @pl.when(mine)
-            def _():
-                pltpu.make_async_copy(wp_ref.at[k, h], q_ref.at[x, y], qr.at[x * NY + y]).start()
-
-            @pl.when(jnp.logical_not(mine))
-            def _():
-                first(k, h).start()
+    def weighting(k, _):
+        e = rem(t + NT - k, NT)
+        here = slot == key_ref[pl.ds(e, 1), :]
+        mix = mix_ref[pl.ds(e, 1), :]
+        high = mix.astype(BF).astype(F32)
+        for i, part in enumerate((high, mix - high)):
+            comb_ref[k, i] = jnp.transpose(jnp.where(here, part, 0.0)).astype(BF)
+        return 0
+
+    lax.fori_loop(0, NT, weighting, 0)
 
     for m in masters:
         m.wait()
@@ -152,15 +129,44 @@
             wp_ref[k, h, 0:COLS, :] = gu[lo:lo + COLS]
             wp_ref[k, h, COLS:PACK, :] = dd[lo:lo + DLO]
 
-        @pl.when(i > 0)
-        def _():
-            j = i - 1
-            first_start(4 + (1 - 2 * rem(j, 2)) * lax.div(j + 1, 2))
-
         return 0
 
     lax.fori_loop(0, NT, pack, 0)
-    first_start(0)
+    pl.semaphore_wait(barrier, count)
+
+    low, base = rem(z, 2), 2 * lax.div(z, 2)
+    peers = {1: base + 1 - low, 2: 2 - base + low, 3: 3 - base - low}
+
+    def tok_copy(i):
+        return send(tok_ref, t_ref.at[z], zs.at[i], zr.at[i], at(g, peers[i], y, t))
+
+    def tok_along(i):
+        return send(tok_ref, ty_ref.at[y], tys.at[i], tyr.at[i], at(g, z, rem(y + i, NY), t))
+
+    for i in (1, 2, 3):
+        tok_copy(i).start()
+    def first(k, h):
+        return send(
+            wp_ref.at[k, h], q_ref.at[x, y], qs.at[k, h], qr.at[x * NY + y],
+            at(g, z, NC * c + h, rem(t + k, NT)),
+        )
+
+    def first_start(k):
+        for h in range(2):
+            mine = (NC * c + h == y) & (rem(t + k, NT) == t)
+
+            @pl.when(mine)
+            def _():
+                pltpu.make_async_copy(wp_ref.at[k, h], q_ref.at[x, y], qr.at[x * NY + y]).start()
+
+            @pl.when(jnp.logical_not(mine))
+            def _():
+                first(k, h).start()
+
+    for k in FARS:
+        first_start(k)
+    for i in (1, 3, 2):
+        tok_along(i).start()
 
     mate, rest = peers[1], 2 - base
     tiles = (mate, pl.ds(rest, 2))
@@ -221,35 +227,45 @@
         return send(q_ref.at[zd], v_ref.at[zz], vs.at[j, q], vr.at[j, q], at(rem(g + q, 2), zd, y, t))
 
     own_v = pltpu.make_async_copy(q_ref.at[z], v_ref.at[zz], vr.at[0, 0])
-
-    def weights_on(j):
-        zd = rem(z + j, NZ)
-        for i in range(NY):
-            send(q_ref.at[zd, i], q_ref.at[zd, i], qs.at[0, 0], qr.at[zd * NY + i], at(g, z, up_y, t)).wait_recv()
-        for q in (1, 0):
-            if j or q:
-                second(j, q).start()
-            else:
-                own_v.start()
+    feeder = lax.div(y, NC)
+    odd = rem(c + feeder, NC)
+
+    def weights_on(i):
+        k = (4, 2, 6, 0)[i] + odd * (-1, 3, -5, 7)[i]
+        zd = lax.div(rem(t + NT - k, NT), NC)
+        for n in range(NY):
+            send(q_ref.at[zd, n], q_ref.at[zd, n], qs.at[0, 0], qr.at[zd * NY + n], at(g, z, up_y, t)).wait_recv()
+        j = rem(zd + NZ - z, NZ)
+        second(j, 1).start()
+
+        @pl.when(j > 0)
+        def _():
+            second(j, 0).start()
+
+        @pl.when(j == 0)
+        def _():
+            own_v.start()
 
     tok_copy(1).wait_recv()
     dispatch(0)
     for k in NEAR[1:]:
         across(0, k).start()
     spread(0, 0)
+    weights_on(0)
+    weights_on(1)
     tok_copy(2).wait_recv()
     tok_copy(3).wait_recv()
     dispatch(1)
     for k in NEAR[1:]:
         across(1, k).start()
     spread(1, 0)
+    weights_on(2)
+    weights_on(3)
     for i in (1, 3, 2):
         tok_along(i).wait_recv()
     dispatch_own()
     for k in FARS[:-1]:
         across(2, k).start()
-    for j in (2, 1, 3, 0):
-        weights_on(j)
     for k in NEAR[1:]:
         spread(0, k)
     for k in NEAR:
@@ -258,17 +274,6 @@
             spread(1, k)
     for k in NEAR:
         forward(1, k)
-
-    def weighting(k, _):
-        e = rem(t + NT - k, NT)
-        here = slot == key_ref[pl.ds(e, 1), :]
-        mix = mix_ref[pl.ds(e, 1), :]
-        high = mix.astype(BF).astype(F32)
-        for i, part in enumerate((high, mix - high)):
-            comb_ref[k, i] = jnp.transpose(jnp.where(here, part, 0.0)).astype(BF)
-        return 0
-
-    lax.fori_loop(0, NT, weighting, 0)
 
     left = lax.broadcasted_iota(I32, (COLS, LANES), 1) < ROWS
 

time: 146 us -> 143 us (0.979)
  Pallas kernels: 145 us -> 143 us
    pallas_call x1, Pallas kernels: 142 us -> 140 us  [local(): pl.pallas_call(kernel, out_shape=shapes, in_specs=[vm, vm, vm, vm, any_,...]
where the time goes in v4:
time: 143 us
  Pallas kernels  143 us (100%)
    pallas_call x1, Pallas kernels, local(): pl.pallas_call(kernel, out_shape=shapes, in_specs=[vm, vm, vm, vm, any_,...  140 us

profile of v4, /device:TPU:64, one launch (start us, length us, event | category | flops | bytes accessed | tf_op | source)
XLA Modules:
  0.0 143.2 jit_solution(14694864460981134996)
XLA Ops:
  0.6 140.0 %handover_kernel.1 = (bf16[512,128]{1,0:T(8,128)(2,1)}, bf16[1,176,2048]{2,1,0:T(8,128)(2,1)}, bf16[1,176,2048]{2,1,0:T(8,128)(2,1)}, bf16[1,176,2048]{2,1,0:T(8,128)(2,1)}) custom-call(bf16[512,128]{1,0:T(8,128)(2,1)} %tok_ref.1, s32[2,512]{1,0:T(2,128)} %bitcast.6, f32[2,512]{1,0:T(2,128)} %bitcast.7, f32[1,64]{1,0:T(1,128)} %bitcast.8, ...), custom_call_target="tpu_custom_call" | custom-call | tf_op jit(solution)/shard_map/handover_kernel/pallas_call | solution.py:535
  140.6 2.6 %output_kernel.1 = (bf16[512,128]{1,0:T(8,128)(2,1)}, bf16[1,176,2048]{2,1,0:T(8,128)(2,1)}, bf16[1,176,2048]{2,1,0:T(8,128)(2,1)}, bf16[1,176,2048]{2,1,0:T(8,128)(2,1)}) custom-call(bf16[512,128]{1,0:T(8,128)(2,1)} %get-tuple-element.12.refs_0_, bf16[1,176,2048]{2,1,0:T(8,128)(2,1)} %get-tuple-element.13.refs_1_, ...), custom_call_target="tpu_custom_call" | custom-call | tf_op jit(solution)/shard_map/output_kernel/pallas_call | solution.py:576

commit v5 on v4

--- a/solution.py
+++ b/solution.py
@@ -114,9 +114,7 @@
         m.wait()
     gain = jnp.concatenate([gain_ref[...], gain_ref[...]], axis=1)
 
-    def pack(i, _):
-        k = 4 + (1 - 2 * rem(i, 2)) * lax.div(i + 1, 2)
-        e = rem(t + k, NT)
+    def pack(e, _):
         pad = jnp.zeros((2 * ROWS, 3 * LANES - WIDTH), F32)
         gu = jnp.concatenate([gm_ref[e], um_ref[e]], axis=0)
         gu = (jnp.transpose(jnp.concatenate([gu, pad], axis=1)) * gain).astype(BF)
@@ -126,8 +124,8 @@
         dd = jnp.transpose(dd).astype(BF)
         for h in range(2):
             lo = h * COLS
-            wp_ref[k, h, 0:COLS, :] = gu[lo:lo + COLS]
-            wp_ref[k, h, COLS:PACK, :] = dd[lo:lo + DLO]
+            wp_ref[e, h, 0:COLS, :] = gu[lo:lo + COLS]
+            wp_ref[e, h, COLS:PACK, :] = dd[lo:lo + DLO]
 
         return 0
 
@@ -145,26 +143,26 @@
 
     for i in (1, 2, 3):
         tok_copy(i).start()
-    def first(k, h):
+    def first(e, h):
         return send(
-            wp_ref.at[k, h], q_ref.at[x, y], qs.at[k, h], qr.at[x * NY + y],
-            at(g, z, NC * c + h, rem(t + k, NT)),
+            wp_ref.at[e, h], q_ref.at[x, y], qs.at[e, h], qr.at[x * NY + y], at(g, z, NC * c + h, e)
         )
 
-    def first_start(k):
-        for h in range(2):
-            mine = (NC * c + h == y) & (rem(t + k, NT) == t)
-
-            @pl.when(mine)
-            def _():
-                pltpu.make_async_copy(wp_ref.at[k, h], q_ref.at[x, y], qr.at[x * NY + y]).start()
-
-            @pl.when(jnp.logical_not(mine))
-            def _():
-                first(k, h).start()
-
-    for k in FARS:
-        first_start(k)
+    def stays(e, h):
+        return (NC * c + h == y) & (e == t)
+
+    for i in range(NX):
+        for n in range(NC):
+            e = NC * rem(x + 2 * NX - z - i, NX) + n
+            for h in range(2):
+                @pl.when(stays(e, h))
+                def _():
+                    pltpu.make_async_copy(wp_ref.at[e, h], q_ref.at[x, y], qr.at[x * NY + y]).start()
+
+                @pl.when(jnp.logical_not(stays(e, h)))
+                def _():
+                    first(e, h).start()
+
     for i in (1, 3, 2):
         tok_along(i).start()
 
@@ -227,12 +225,9 @@
         return send(q_ref.at[zd], v_ref.at[zz], vs.at[j, q], vr.at[j, q], at(rem(g + q, 2), zd, y, t))
 
     own_v = pltpu.make_async_copy(q_ref.at[z], v_ref.at[zz], vr.at[0, 0])
-    feeder = lax.div(y, NC)
-    odd = rem(c + feeder, NC)
 
     def weights_on(i):
-        k = (4, 2, 6, 0)[i] + odd * (-1, 3, -5, 7)[i]
-        zd = lax.div(rem(t + NT - k, NT), NC)
+        zd = rem(x + z + i, NX)
         for n in range(NY):
             send(q_ref.at[zd, n], q_ref.at[zd, n], qs.at[0, 0], qr.at[zd * NY + n], at(g, z, up_y, t)).wait_recv()
         j = rem(zd + NZ - z, NZ)
@@ -261,17 +256,17 @@
     spread(1, 0)
     weights_on(2)
     weights_on(3)
+    for k in NEAR[1:]:
+        spread(0, k)
     for i in (1, 3, 2):
         tok_along(i).wait_recv()
     dispatch_own()
-    for k in FARS[:-1]:
-        across(2, k).start()
-    for k in NEAR[1:]:
-        spread(0, k)
     for k in NEAR:
         forward(0, k)
         if k:
             spread(1, k)
+    for k in FARS[:-1]:
+        across(2, k).start()
     for k in NEAR:
         forward(1, k)
 
@@ -473,14 +468,11 @@
         tok_copy(i).wait_send()
         tok_along(i).wait_send()
         token_sum(i).wait_send()
-    for k in range(NT):
+    for e in range(NT):
         for h in range(2):
-            if k:
-                first(k, h).wait_send()
-            else:
-                @pl.when(NC * c + h != y)
-                def _():
-                    first(k, h).wait_send()
+            @pl.when(jnp.logical_not(stays(e, h)))
+            def _():
+                first(e, h).wait_send()
     for j in range(NZ):
         for q in range(2):
             if j or q:

time: 143 us -> 138 us (0.965)
  Pallas kernels: 143 us -> 137 us
    pallas_call x1, Pallas kernels: 140 us -> 135 us  [local(): pl.pallas_call(kernel, out_shape=shapes, in_specs=[vm, vm, vm, vm, any_,...]
where the time goes in v5:
time: 138 us
  Pallas kernels  137 us (99%)
    pallas_call x1, Pallas kernels, local(): pl.pallas_call(kernel, out_shape=shapes, in_specs=[vm, vm, vm, vm, any_,...  135 us

profile of v5, /device:TPU:64, one launch (start us, length us, event | category | flops | bytes accessed | tf_op | source)
XLA Modules:
  0.0 137.8 jit_solution(350186435292127860)
XLA Ops:
  0.6 134.5 %handover_kernel.1 = (bf16[512,128]{1,0:T(8,128)(2,1)}, bf16[1,176,2048]{2,1,0:T(8,128)(2,1)}, bf16[1,176,2048]{2,1,0:T(8,128)(2,1)}, bf16[1,176,2048]{2,1,0:T(8,128)(2,1)}) custom-call(bf16[512,128]{1,0:T(8,128)(2,1)} %tok_ref.1, s32[2,512]{1,0:T(2,128)} %bitcast.6, f32[2,512]{1,0:T(2,128)} %bitcast.7, f32[1,64]{1,0:T(1,128)} %bitcast.8, ...), custom_call_target="tpu_custom_call" | custom-call | tf_op jit(solution)/shard_map/handover_kernel/pallas_call | solution.py:527
  135.2 2.6 %output_kernel.1 = (bf16[512,128]{1,0:T(8,128)(2,1)}, bf16[1,176,2048]{2,1,0:T(8,128)(2,1)}, bf16[1,176,2048]{2,1,0:T(8,128)(2,1)}, bf16[1,176,2048]{2,1,0:T(8,128)(2,1)}) custom-call(bf16[512,128]{1,0:T(8,128)(2,1)} %get-tuple-element.12.refs_0_, bf16[1,176,2048]{2,1,0:T(8,128)(2,1)} %get-tuple-element.13.refs_1_, ...), custom_call_target="tpu_custom_call" | custom-call | tf_op jit(solution)/shard_map/output_kernel/pallas_call | solution.py:568

commit v6 on v5

--- a/solution.py
+++ b/solution.py
@@ -20,8 +20,8 @@
 WIDTH = 352
 COLS = 176
 LANES = 128
-DLO, DHI = 96, 80
-PACK = COLS + DLO
+DOWN = COLS // 2
+PACK = COLS + DOWN
 TOK = 512
 FEAT = 128
 MODEL = 2048
@@ -117,15 +117,14 @@
     def pack(e, _):
         pad = jnp.zeros((2 * ROWS, 3 * LANES - WIDTH), F32)
         gu = jnp.concatenate([gm_ref[e], um_ref[e]], axis=0)
-        gu = (jnp.transpose(jnp.concatenate([gu, pad], axis=1)) * gain).astype(BF)
+        gu = jnp.transpose(jnp.concatenate([gu, pad], axis=1)) * gain
         dn = dm_ref[e]
         dn = jnp.concatenate([dn, pad[:ROWS]], axis=1)
-        dd = jnp.concatenate([dn, pltpu.roll(dn, 3 * LANES - DLO, 1)], axis=0)
-        dd = jnp.transpose(dd).astype(BF)
+        dd = jnp.concatenate([dn, pltpu.roll(dn, 3 * LANES - DOWN, 1)], axis=0)
+        dd = jnp.transpose(dd)
         for h in range(2):
             lo = h * COLS
-            wp_ref[e, h, 0:COLS, :] = gu[lo:lo + COLS]
-            wp_ref[e, h, COLS:PACK, :] = dd[lo:lo + DLO]
+            wp_ref[e, h] = jnp.concatenate([gu[lo:lo + COLS], dd[lo:lo + DOWN]], axis=0).astype(BF)
 
         return 0
 
@@ -151,20 +150,28 @@
     def stays(e, h):
         return (NC * c + h == y) & (e == t)
 
-    for i in range(NX):
-        for n in range(NC):
-            e = NC * rem(x + 2 * NX - z - i, NX) + n
-            for h in range(2):
-                @pl.when(stays(e, h))
-                def _():
-                    pltpu.make_async_copy(wp_ref.at[e, h], q_ref.at[x, y], qr.at[x * NY + y]).start()
-
-                @pl.when(jnp.logical_not(stays(e, h)))
-                def _():
-                    first(e, h).start()
-
-    for i in (1, 3, 2):
-        tok_along(i).start()
+    def pieces(i):
+        return [(NC * rem(x + 2 * NX - z - i, NX) + n, h) for n in range(NC) for h in range(2)]
+
+    def wave(i):
+        for e, h in pieces(i):
+            @pl.when(stays(e, h))
+            def _():
+                pltpu.make_async_copy(wp_ref.at[e, h], q_ref.at[x, y], qr.at[x * NY + y]).start()
+
+            @pl.when(jnp.logical_not(stays(e, h)))
+            def _():
+                first(e, h).start()
+
+    def wave_left(i):
+        for e, h in pieces(i):
+            @pl.when(jnp.logical_not(stays(e, h)))
+            def _():
+                first(e, h).wait_send()
+
+    wave(0)
+    wave(1)
+
 
     mate, rest = peers[1], 2 - base
     tiles = (mate, pl.ds(rest, 2))
@@ -246,7 +253,13 @@
     for k in NEAR[1:]:
         across(0, k).start()
     spread(0, 0)
+    wave_left(0)
+    wave(2)
     weights_on(0)
+    wave_left(1)
+    wave(3)
+    for i in (1, 3, 2):
+        tok_along(i).start()
     weights_on(1)
     tok_copy(2).wait_recv()
     tok_copy(3).wait_recv()
@@ -279,8 +292,9 @@
             cols = pl.ds(pl.multiple_of((zs_ * (NY // 2) + i) * LANES, LANES), LANES)
             gate_ref[:, cols] = jnp.where(left, a[:COLS], rb[:COLS]).astype(BF)
             up_ref[:, cols] = jnp.where(left, ra[:COLS], b[:COLS]).astype(BF)
-            down_ref[0:DLO, cols] = jnp.where(left[:DLO], a[COLS:], rb[COLS:]).astype(BF)
-            down_ref[DLO:COLS, cols] = jnp.where(left[:DHI], ra[COLS:COLS + DHI], b[COLS:COLS + DHI]).astype(BF)
+            down_ref[:, cols] = jnp.concatenate(
+                [jnp.where(left[:DOWN], a[COLS:], rb[COLS:]), jnp.where(left[:DOWN], ra[COLS:], b[COLS:])], axis=0
+            ).astype(BF)
 
     own_v.wait()
     unpack(zz)
@@ -468,11 +482,8 @@
         tok_copy(i).wait_send()
         tok_along(i).wait_send()
         token_sum(i).wait_send()
-    for e in range(NT):
-        for h in range(2):
-            @pl.when(jnp.logical_not(stays(e, h)))
-            def _():
-                first(e, h).wait_send()
+    wave_left(2)
+    wave_left(3)
     for j in range(NZ):
         for q in range(2):
             if j or q:

time: 138 us -> 136 us (0.986)
  Pallas kernels: 137 us -> 135 us
    pallas_call x1, Pallas kernels: 135 us -> 132 us  [local(): pl.pallas_call(kernel, out_shape=shapes, in_specs=[vm, vm, vm, vm, any_,...]
where the time goes in v6:
time: 136 us
  Pallas kernels  135 us (99%)
    pallas_call x1, Pallas kernels, local(): pl.pallas_call(kernel, out_shape=shapes, in_specs=[vm, vm, vm, vm, any_,...  132 us

profile of v6, /device:TPU:64, one launch (start us, length us, event | category | flops | bytes accessed | tf_op | source)
XLA Modules:
  0.0 135.7 jit_solution(7819077809782838835)
XLA Ops:
  0.6 132.5 %handover_kernel.1 = (bf16[512,128]{1,0:T(8,128)(2,1)}, bf16[1,176,2048]{2,1,0:T(8,128)(2,1)}, bf16[1,176,2048]{2,1,0:T(8,128)(2,1)}, bf16[1,176,2048]{2,1,0:T(8,128)(2,1)}) custom-call(bf16[512,128]{1,0:T(8,128)(2,1)} %tok_ref.1, s32[2,512]{1,0:T(2,128)} %bitcast.6, f32[2,512]{1,0:T(2,128)} %bitcast.7, f32[1,64]{1,0:T(1,128)} %bitcast.8, ...), custom_call_target="tpu_custom_call" | custom-call | tf_op jit(solution)/shard_map/handover_kernel/pallas_call | solution.py:538
  133.1 2.6 %output_kernel.1 = (bf16[512,128]{1,0:T(8,128)(2,1)}, bf16[1,176,2048]{2,1,0:T(8,128)(2,1)}, bf16[1,176,2048]{2,1,0:T(8,128)(2,1)}, bf16[1,176,2048]{2,1,0:T(8,128)(2,1)}) custom-call(bf16[512,128]{1,0:T(8,128)(2,1)} %get-tuple-element.12.refs_0_, bf16[1,176,2048]{2,1,0:T(8,128)(2,1)} %get-tuple-element.13.refs_1_, ...), custom_call_target="tpu_custom_call" | custom-call | tf_op jit(solution)/shard_map/output_kernel/pallas_call | solution.py:579

commit v7 on v6

--- a/solution.py
+++ b/solution.py
@@ -140,8 +140,6 @@
     def tok_along(i):
         return send(tok_ref, ty_ref.at[y], tys.at[i], tyr.at[i], at(g, z, rem(y + i, NY), t))
 
-    for i in (1, 2, 3):
-        tok_copy(i).start()
     def first(e, h):
         return send(
             wp_ref.at[e, h], q_ref.at[x, y], qs.at[e, h], qr.at[x * NY + y], at(g, z, NC * c + h, e)
@@ -169,8 +167,11 @@
             def _():
                 first(e, h).wait_send()
 
+    tok_copy(1).start()
     wave(0)
     wave(1)
+    tok_copy(2).start()
+    tok_copy(3).start()
 
 
     mate, rest = peers[1], 2 - base
@@ -249,12 +250,12 @@
             own_v.start()
 
     tok_copy(1).wait_recv()
+    wave_left(0)
+    wave(2)
     dispatch(0)
     for k in NEAR[1:]:
         across(0, k).start()
     spread(0, 0)
-    wave_left(0)
-    wave(2)
     weights_on(0)
     wave_left(1)
     wave(3)
@@ -365,9 +366,9 @@
         k = kth(i)
         experts(k)
         products(0, k)
-        late = product(LATE, k)
         far(0, k).start()
         plain(0, k).start()
+        late = product(LATE, k)
 
         @pl.when(k > 0)
         def _():

time: 136 us -> 135 us (level)
  no operation moved by 1% of the time
where the time goes in v7:
time: 135 us
  Pallas kernels  134 us (99%)
    pallas_call x1, Pallas kernels, local(): pl.pallas_call(kernel, out_shape=shapes, in_specs=[vm, vm, vm, vm, any_,...  132 us

profile of v7, /device:TPU:64, one launch (start us, length us, event | category | flops | bytes accessed | tf_op | source)
XLA Modules:
  0.0 134.9 jit_solution(4435184899217785148)
XLA Ops:
  0.6 131.6 %handover_kernel.1 = (bf16[512,128]{1,0:T(8,128)(2,1)}, bf16[1,176,2048]{2,1,0:T(8,128)(2,1)}, bf16[1,176,2048]{2,1,0:T(8,128)(2,1)}, bf16[1,176,2048]{2,1,0:T(8,128)(2,1)}) custom-call(bf16[512,128]{1,0:T(8,128)(2,1)} %tok_ref.1, s32[2,512]{1,0:T(2,128)} %bitcast.6, f32[2,512]{1,0:T(2,128)} %bitcast.7, f32[1,64]{1,0:T(1,128)} %bitcast.8, ...), custom_call_target="tpu_custom_call" | custom-call | tf_op jit(solution)/shard_map/handover_kernel/pallas_call | solution.py:539
  132.3 2.6 %output_kernel.1 = (bf16[512,128]{1,0:T(8,128)(2,1)}, bf16[1,176,2048]{2,1,0:T(8,128)(2,1)}, bf16[1,176,2048]{2,1,0:T(8,128)(2,1)}, bf16[1,176,2048]{2,1,0:T(8,128)(2,1)}) custom-call(bf16[512,128]{1,0:T(8,128)(2,1)} %get-tuple-element.12.refs_0_, bf16[1,176,2048]{2,1,0:T(8,128)(2,1)} %get-tuple-element.13.refs_1_, ...), custom_call_target="tpu_custom_call" | custom-call | tf_op jit(solution)/shard_map/output_kernel/pallas_call | solution.py:580
